TPU v7x, 256 devices: a whole 4x4x8 slice. The times are simulated.
256 devices in a mesh: ep: 64 (over z, x, core), tp: 4 (over y).
Axes of the slice: x: 4, y: 4, z: 8, core: 2. Of those that a mesh axis runs over, the one named last changes fastest.
Arguments:
- first_micro_values: bfloat16 [65536, 2048], P('ep', 'tp'), may hold values from -6 to 6
- group_state_maps: bfloat16 [2, 65536, 1024], P(None, 'ep', 'tp'), may hold values from -6 to 6
- gate_preactivation: bfloat16 [65536, 2048], P('ep', 'tp'), may hold values from -6 to 6
- step_preactivation: float32 [65536, 32], P('ep', 'tp'), may hold values from -5.7 to 5.7
- head_step_bias: float32 [32], P('tp'), may hold values from -12 to -3
- head_log_decay: float32 [32], P('tp'), may hold values from -12 to 1
- decay_increment: float32 [65536, 32], P('ep', 'tp'), may hold values from -1.4 to 0
- head_direct_gain: float32 [32], P('tp'), may hold values from 0.1 to 1.9
- convolution_value_taps: bfloat16 [4, 2048], P(None, 'tp'), may hold values from -3 to 3
- convolution_map_taps: bfloat16 [2, 4, 1024], P(None, None, 'tp'), may hold values from -3 to 3
- grouped_norm_gain: float32 [2048], P('tp'), may hold values from 0.1 to 1.9
- second_micro_tokens: bfloat16 [65536, 2048], P(('ep', 'tp')), may hold values from -6 to 6
- expert_norm_gain: float32 [2048], replicated, may hold values from 0.1 to 1.9
- routes: int32 [65536, 2], P(('ep', 'tp')), may hold values from 0 to 63, all different within a row; in each aligned block of 256 rows (0 to 255, 256 to 511, ...) at most 12 rows name the same one
- visit_weight: float32 [65536, 2], P(('ep', 'tp')), may hold values from 0.1 to 1
- gate_weight_table: bfloat16 [64, 2048, 1024], P('ep', None, 'tp'), may hold values from -0.125 to 0.125
- up_weight_table: bfloat16 [64, 2048, 1024], P('ep', None, 'tp'), may hold values from -0.125 to 0.125
- down_weight_table: bfloat16 [64, 2048, 1024], P('ep', None, 'tp'), may hold values from -0.1875 to 0.1875
Outputs:
- mixer_gated_output: bfloat16 [65536, 2048], P('ep', 'tp')
- routed_out: bfloat16 [65536, 2048], P(('ep', 'tp'))
Inputs may be any that keep to these rules, and one draw needn't show every extreme that they name: `routes`: A row names 2 different experts. In each aligned block of 256 rows (the rows of one device), no expert is named by more than 12 rows, a bound that some block reaches.
All inputs are finite; a program needn't handle non-finite values.
Results may differ from a plain program's by a relative error of at most 0.0071.
Values may be sent and summed in bfloat16 or wider, within the bound.
A program may use at most 128 MiB of HBM per device.

v0:
```python
import jax
import jax.numpy as jnp
from jax import lax
from jax.experimental import pallas as pl
from jax.experimental.pallas import tpu as pltpu
from jax.sharding import Mesh
from jax.sharding import PartitionSpec as P

HEADDIM = 64
NSTATE = 128
BLOCK = 128
EP = ("ep_0", "ep_1", "ep_2")
EP_TP = ("ep_0", "ep_1", "ep_2", "tp")


EPSILON = 1e-05
CONTRACT_LAST = (((1,), (1,)), ((), ()))


def shifted(block, axis, distance):
    devices = range(lax.axis_size(axis))
    route = [(i - distance, i) for i in devices if i - distance in devices]
    return lax.ppermute(block, axis, route)


def nothing_yet(x, identity):
    return jax.tree.map(
        lambda part, zero: jnp.zeros_like(part) + jnp.asarray(zero, part.dtype), x, identity
    )


def entering_2(x, axes, combine, identity):
    before = start = nothing_yet(x, identity)
    total = x
    for axis in reversed(axes):
        count, mine = (lax.axis_size(axis), lax.axis_index(axis))
        pieces = jax.tree.map(lambda part: lax.all_gather(part, axis), total)
        inside, total = (start, start)
        for k in range(count):
            passed = k < mine
            total = combine(total, jax.tree.map(lambda part: part[k], pieces))
            inside = jax.tree.map(lambda new, old: jnp.where(passed, new, old), total, inside)
        before = combine(inside, before)
    return before


def causal_conv(before, values, weights):
    length = values.shape[0]
    kernel = weights.shape[0]
    padded = jnp.concatenate([before, values], axis=0).astype(jnp.float32)
    summed_total = jnp.zeros(values.shape, jnp.float32)
    for offset in range(kernel):
        summed_total = (
            summed_total + weights[offset].astype(jnp.float32) * padded[offset : offset + length]
        )
    return jax.nn.silu(summed_total)


def combine_states(earlier, later):
    return (earlier[0] * later[0], earlier[1] * later[0][..., None, None] + later[1])


def mixer_half(
    first_micro_values,
    group_state_maps,
    gate_preactivation,
    step_preactivation,
    head_step_bias,
    head_log_decay,
    decay_increment,
    head_direct_gain,
    convolution_value_taps,
    convolution_map_taps,
    grouped_norm_gain,
):
    length, channels = first_micro_values.shape
    head_count = step_preactivation.shape[1]
    maps_width = group_state_maps.shape[2]
    groups = maps_width // NSTATE
    per_group = head_count // groups
    blocks = length // BLOCK
    conv_reach = convolution_value_taps.shape[0] - 1
    tail_rows = jnp.concatenate(
        [
            first_micro_values[length - conv_reach :],
            group_state_maps[0, length - conv_reach :],
            group_state_maps[1, length - conv_reach :],
        ],
        axis=1,
    )
    before = shifted(tail_rows, EP, 1)
    conv_out = causal_conv(before[:, :channels], first_micro_values, convolution_value_taps)
    in_maps = causal_conv(
        before[:, channels : channels + maps_width], group_state_maps[0], convolution_map_taps[0]
    )
    out_maps = causal_conv(
        before[:, channels + maps_width :], group_state_maps[1], convolution_map_taps[1]
    )
    step_length = jax.nn.softplus(step_preactivation + head_step_bias)
    decay_logarithm = -jnp.exp(head_log_decay) * step_length + decay_increment
    head_values = conv_out.reshape(blocks, BLOCK, groups, per_group, HEADDIM)
    scaled_values = head_values * step_length.reshape(blocks, BLOCK, groups, per_group)[..., None]
    in_blocks = in_maps.reshape(blocks, BLOCK, groups, NSTATE)
    out_blocks = out_maps.reshape(blocks, BLOCK, groups, NSTATE)
    running = jnp.cumsum(decay_logarithm.reshape(blocks, BLOCK, groups, per_group), axis=1)
    causal = jnp.tril(jnp.ones((BLOCK, BLOCK), dtype=bool))
    scores = jnp.einsum("blgn,bsgn->bgls", out_blocks, in_blocks)
    ordered = jnp.moveaxis(running, 1, -1)
    between = jnp.exp(jnp.where(causal, ordered[..., :, None] - ordered[..., None, :], -jnp.inf))
    inside = jnp.einsum("bgrls,bsgrp->blgrp", scores[:, :, None] * between, scaled_values)
    block_total = running[:, -1]
    to_end = jnp.exp(block_total[:, None] - running)
    block_states = jnp.einsum("blgn,blgr,blgrp->bgrpn", in_blocks, to_end, scaled_values)

    def carry_block(carry_state, inputs):
        return (carry_state * jnp.exp(inputs[1])[..., None, None] + inputs[0], carry_state)

    zero_state = jnp.zeros((groups, per_group, HEADDIM, NSTATE), jnp.float32)
    local_end, local_enter = lax.scan(carry_block, zero_state, (block_states, block_total))
    device_decay = jnp.exp(jnp.sum(block_total, axis=0))
    identity = (jnp.ones_like(device_decay), jnp.zeros_like(local_end))
    unused, incoming = entering_2((device_decay, local_end), EP, combine_states, identity)
    prefix = jnp.exp(jnp.cumsum(block_total, axis=0) - block_total)
    entering = local_enter + prefix[..., None, None] * incoming[None]
    carried = jnp.einsum("blgn,bgrpn->blgrp", out_blocks, entering)
    carried = carried * jnp.exp(running)[..., None]
    mixed_out = (
        inside + carried + head_values * head_direct_gain.reshape(groups, per_group)[:, :, None]
    )
    gated_out = mixed_out.reshape(length, channels) * jax.nn.silu(
        gate_preactivation.astype(jnp.float32)
    )
    grouped = gated_out.reshape(length, groups, channels // groups)
    normed = grouped * lax.rsqrt(jnp.mean(grouped * grouped, axis=-1, keepdims=True) + EPSILON)
    return (normed.reshape(length, channels) * grouped_norm_gain).astype(jnp.bfloat16)


SLOTS = 12
ORDER = (4, 1, 7, 3, 5, 2, 6, 0)
MESH_IDS = pl.DeviceIdType.MESH


def here():
    return (lax.axis_index("ep_0"), lax.axis_index("ep_1"), lax.axis_index("ep_2"))


def beside(step):
    return {"tp": lax.rem(lax.axis_index("tp") + step, 4)}


def ep_target(place, dz, dxc):
    z, x, c = place
    tz = lax.rem(z + dz, 8)
    tx = lax.rem(x + lax.div(dxc, 2), 4)
    tc = lax.rem(c + lax.rem(dxc, 2), 2)
    return tz * 8 + tx * 2 + tc, {"ep_0": tz, "ep_1": tx, "ep_2": tc}


def for_all_peers(act):
    place = here()

    def some(dxc, unused):
        for dz in ORDER:
            act(*ep_target(place, dz, dxc))
        return unused

    for dz in ORDER:
        if dz:
            act(*ep_target(place, dz, 0))
    lax.fori_loop(1, 8, some, 0)


def exchange(source, landing, send_sem, recv_sem):
    z, x, c = here()
    me = z * 8 + x * 2 + c

    def send(index, device):
        pltpu.make_async_remote_copy(
            src_ref=source.at[index],
            dst_ref=landing.at[me],
            send_sem=send_sem,
            recv_sem=recv_sem,
            device_id=device,
            device_id_type=MESH_IDS,
        ).start()

    for_all_peers(send)


def all_but_one(source, landing, send_sem, recv_sem):
    return pltpu.make_async_remote_copy(
        src_ref=source.at[pl.ds(0, 63)],
        dst_ref=landing.at[pl.ds(0, 63)],
        send_sem=send_sem,
        recv_sem=recv_sem,
        device_id=beside(1),
        device_id_type=MESH_IDS,
    )


def floor_div(values, divisor):
    return jnp.floor((values + 0.5) * (1.0 / divisor))


def iota(shape, axis):
    return lax.broadcasted_iota(jnp.int32, shape, axis).astype(jnp.float32)


def dot(a, b):
    return jnp.dot(a, b, preferred_element_type=jnp.float32)


def repack_matrix():
    size = 16 * SLOTS
    row = iota((size, size), 0)
    outer = floor_div(row, 4 * SLOTS)
    rest = row - 4 * SLOTS * outer
    inner = floor_div(rest, SLOTS)
    partner = inner * (4 * SLOTS) + outer * SLOTS + (rest - inner * SLOTS)
    return jnp.where(iota((size, size), 1) == partner, 1.0, 0.0).astype(jnp.bfloat16)


def pack_rows(source, landing, matrix, width):
    def group(g, unused):
        rows = source[pl.ds(pl.multiple_of(g * 48, 16), 48), :]
        tall = jnp.concatenate([rows[:, p * width : (p + 1) * width] for p in range(4)], axis=0)
        landing[pl.ds(g * 4, 4)] = dot(matrix, tall).astype(jnp.bfloat16).reshape(4, 48, width)
        return unused

    lax.fori_loop(0, 16, group, 0)


def unpack_rows(source, landing, matrix, width):
    def group(g, unused):
        tall = source[pl.ds(g * 4, 4)].reshape(192, width)
        rows = dot(matrix, tall).astype(jnp.bfloat16)
        for p in range(4):
            landing[pl.ds(pl.multiple_of(g * 48, 16), 48), p * width : (p + 1) * width] = rows[
                p * 48 : (p + 1) * 48
            ]
        return unused

    lax.fori_loop(0, 16, group, 0)


class Neighbours:
    def __init__(self, own, slots, send_sems, recv_sems, first, start, size):
        half = size // 2
        whole, low, high = pl.ds(start, size), pl.ds(start, half), pl.ds(start + half, half)

        def copy(which, source, landing, step):
            return pltpu.make_async_remote_copy(
                src_ref=source,
                dst_ref=landing,
                send_sem=send_sems.at[first + which],
                recv_sem=recv_sems.at[first + which],
                device_id=beside(step),
                device_id_type=MESH_IDS,
            )

        self.near = (
            copy(0, own.at[0, whole], slots.at[1, whole], 1),
            copy(1, own.at[0, whole], slots.at[2, whole], 3),
        )
        self.far = (
            copy(2, slots.at[1, low], slots.at[3, low], 1),
            copy(3, slots.at[2, high], slots.at[3, high], 3),
        )

    def start(self):
        for copy in self.near:
            copy.start()

    def forward(self):
        for arrived, onward in zip(self.near, self.far):
            arrived.wait_recv()
            onward.start()

    def arrive(self):
        for copy in self.far:
            copy.wait_recv()

    def drain(self):
        for copy in self.near + self.far:
            copy.wait_send()


def routed_kernel(
    tokens_hbm,
    gain_ref,
    routes_ref,
    weight_ref,
    gate_hbm,
    up_hbm,
    down_hbm,
    out_ref,
    tokens,
    normed,
    choice,
    mix_high,
    mix_low,
    rows_ref,
    sent,
    landed,
    hidden,
    answers,
    returned,
    gate,
    up,
    down,
    local_sems,
    near_send,
    near_recv,
    dispatch_sems,
    answer_send,
    answer_recv,
):
    own_copies = [
        pltpu.make_async_copy(tokens_hbm, tokens, local_sems.at[0]),
        pltpu.make_async_copy(gate_hbm.at[0], gate.at[0], local_sems.at[1]),
        pltpu.make_async_copy(up_hbm.at[0], up.at[0], local_sems.at[2]),
        pltpu.make_async_copy(down_hbm.at[0], down.at[0], local_sems.at[3]),
    ]
    for copy in own_copies:
        copy.start()
    barrier = pltpu.get_barrier_semaphore()

    def greet(unused, device):
        pl.semaphore_signal(barrier, inc=1, device_id=device, device_id_type=MESH_IDS)

    for step in (1, 3):
        greet(0, beside(step))
    for_all_peers(greet)
    pl.semaphore_wait(barrier, 65)

    gate_near = Neighbours(gate_hbm, gate, near_send, near_recv, 0, 0, 2048)
    up_near = Neighbours(up_hbm, up, near_send, near_recv, 4, 0, 2048)
    down_near = [
        Neighbours(down_hbm, down, near_send, near_recv, 8 + 4 * p, p * 512, 512) for p in range(4)
    ]
    gate_near.start()
    up_near.start()

    own_copies[0].wait()

    def norm_rows(i, unused):
        rows = pl.ds(pl.multiple_of(i * 32, 32), 32)
        values = tokens[rows, :].astype(jnp.float32)
        centered = values - jnp.mean(values, axis=1, keepdims=True)
        scale = lax.rsqrt(jnp.mean(centered * centered, axis=1, keepdims=True) + EPSILON)
        normed[rows, :] = (centered * scale * gain_ref[...]).astype(jnp.bfloat16)
        return unused

    lax.fori_loop(0, 8, norm_rows, 0)

    experts = lax.broadcasted_iota(jnp.int32, (256, 64), 1)
    hits = [jnp.where(routes_ref[:, k : k + 1] == experts, 1.0, 0.0) for k in range(2)]
    named = hits[0] + hits[1]
    earlier = jnp.where(iota((256, 256), 0) > iota((256, 256), 1), 1.0, 0.0).astype(jnp.bfloat16)
    place = dot(earlier, named.astype(jnp.bfloat16))
    key = jnp.where(named > 0.5, place, -1.0)
    key_rows = jnp.transpose(key).astype(jnp.bfloat16)
    slot_rows = iota((768, 64), 0)
    spread = jnp.where(floor_div(slot_rows, SLOTS) == iota((768, 64), 1), 1.0, 0.0)
    spread = spread.astype(jnp.bfloat16)
    wanted = iota((768, 256), 0)
    wanted = wanted - SLOTS * floor_div(wanted, SLOTS)
    choice[...] = jnp.where(dot(spread, key_rows) == wanted, 1.0, 0.0).astype(jnp.bfloat16)
    matrix = repack_matrix()

    def pick(p, unused):
        columns = pl.ds(pl.multiple_of(p * 512, 512), 512)
        rows_ref[:, columns] = dot(choice[...], normed[:, columns]).astype(jnp.bfloat16)
        return unused

    lax.fori_loop(0, 4, pick, 0)
    pack_rows(rows_ref, sent, matrix, 512)
    exchange(sent, landed, dispatch_sems.at[0], dispatch_sems.at[1])
    z, x, c = here()
    me = z * 8 + x * 2 + c
    landed[me] = sent[me]

    weights = weight_ref[:, 0:1] * hits[0] + weight_ref[:, 1:2] * hits[1]
    columns = iota((64, 768), 1)
    spread_columns = jnp.where(floor_div(columns, SLOTS) == iota((64, 768), 0), 1.0, 0.0)
    spread_columns = spread_columns.astype(jnp.bfloat16)
    wanted = iota((256, 768), 1)
    wanted = wanted - SLOTS * floor_div(wanted, SLOTS)
    mine = dot(key.astype(jnp.bfloat16), spread_columns) == wanted
    high = weights.astype(jnp.bfloat16)
    low = (weights - high.astype(jnp.float32)).astype(jnp.bfloat16)
    mix_high[...] = jnp.where(mine, dot(high, spread_columns), 0.0).astype(jnp.bfloat16)
    mix_low[...] = jnp.where(mine, dot(low, spread_columns), 0.0).astype(jnp.bfloat16)

    gate_near.forward()
    up_near.forward()
    for part in down_near:
        part.start()
    gate_near.arrive()
    up_near.arrive()
    for part in down_near:
        part.forward()
    for copy in own_copies[1:]:
        copy.wait()

    all_but_one(sent, landed, dispatch_sems.at[0], dispatch_sems.at[1]).wait()
    unpack_rows(landed, rows_ref, matrix, 512)

    def activate(j, unused):
        for r in range(3):
            rows = rows_ref[r * 256 : (r + 1) * 256, :]
            opened = dot(rows, gate[j])
            raised = dot(rows, up[j])
            hidden[j, r * 256 : (r + 1) * 256, :] = (jax.nn.silu(opened) * raised).astype(
                jnp.bfloat16
            )
        return unused

    lax.fori_loop(0, 4, activate, 0)

    for p in range(4):
        down_near[p].arrive()

        def answer(n, unused):
            lines = pl.ds(pl.multiple_of(p * 512 + n * 256, 256), 256)
            total = jnp.zeros((768, 256), jnp.float32)
            for j in range(4):
                total = total + lax.dot_general(
                    hidden[j], down[j, lines, :], CONTRACT_LAST, preferred_element_type=jnp.float32
                )
            rows_ref[:, lines] = total.astype(jnp.bfloat16)
            return unused

        lax.fori_loop(0, 2, answer, 0)
        pack_rows(rows_ref.at[:, pl.ds(p * 512, 512)], answers.at[p], matrix, 128)
        exchange(answers.at[p], returned.at[p], answer_send.at[p], answer_recv.at[p])
        returned[p, me] = answers[p, me]

    for p in range(4):
        all_but_one(answers.at[p], returned.at[p], answer_send.at[p], answer_recv.at[p]).wait()
        lines = pl.ds(p * 512, 512)
        unpack_rows(returned.at[p], rows_ref.at[:, lines], matrix, 128)
        out_ref[:, lines] = (
            dot(mix_high[...], rows_ref[:, lines]) + dot(mix_low[...], rows_ref[:, lines])
        ).astype(jnp.bfloat16)

    for near in [gate_near, up_near] + down_near:
        near.drain()


def routed_half(
    second_micro_tokens,
    expert_norm_gain,
    routes,
    visit_weight,
    gate_weight_table,
    up_weight_table,
    down_weight_table,
):
    vmem = pl.BlockSpec(memory_space=pltpu.VMEM)
    hbm = pl.BlockSpec(memory_space=pl.ANY)
    bf16 = jnp.bfloat16
    return pl.pallas_call(
        routed_kernel,
        out_shape=jax.ShapeDtypeStruct((256, 2048), bf16),
        in_specs=[hbm, vmem, vmem, vmem, hbm, hbm, hbm],
        out_specs=vmem,
        scratch_shapes=[
            pltpu.VMEM((256, 2048), bf16),
            pltpu.VMEM((256, 2048), bf16),
            pltpu.VMEM((768, 256), bf16),
            pltpu.VMEM((256, 768), bf16),
            pltpu.VMEM((256, 768), bf16),
            pltpu.VMEM((768, 2048), bf16),
            pltpu.VMEM((64, 48, 512), bf16),
            pltpu.VMEM((64, 48, 512), bf16),
            pltpu.VMEM((4, 768, 256), bf16),
            pltpu.VMEM((4, 64, 48, 128), bf16),
            pltpu.VMEM((4, 64, 48, 128), bf16),
            pltpu.VMEM((4, 2048, 256), bf16),
            pltpu.VMEM((4, 2048, 256), bf16),
            pltpu.VMEM((4, 2048, 256), bf16),
            pltpu.SemaphoreType.DMA((4,)),
            pltpu.SemaphoreType.DMA((24,)),
            pltpu.SemaphoreType.DMA((24,)),
            pltpu.SemaphoreType.DMA((2,)),
            pltpu.SemaphoreType.DMA((4,)),
            pltpu.SemaphoreType.DMA((4,)),
        ],
        compiler_params=pltpu.CompilerParams(
            collective_id=0, has_side_effects=True, vmem_limit_bytes=60 * 2**20
        ),
        cost_estimate=pl.CostEstimate(
            flops=10**10, bytes_accessed=2 * 10**7, transcendentals=10**6
        ),
    )(
        second_micro_tokens,
        expert_norm_gain.reshape(1, -1),
        routes,
        visit_weight,
        gate_weight_table,
        up_weight_table,
        down_weight_table,
    )


def body(
    first_micro_values,
    group_state_maps,
    gate_preactivation,
    step_preactivation,
    head_step_bias,
    head_log_decay,
    decay_increment,
    head_direct_gain,
    convolution_value_taps,
    convolution_map_taps,
    grouped_norm_gain,
    second_micro_tokens,
    expert_norm_gain,
    routes,
    visit_weight,
    gate_weight_table,
    up_weight_table,
    down_weight_table,
):
    mixer_gated_output = mixer_half(
        first_micro_values,
        group_state_maps,
        gate_preactivation,
        step_preactivation,
        head_step_bias,
        head_log_decay,
        decay_increment,
        head_direct_gain,
        convolution_value_taps,
        convolution_map_taps,
        grouped_norm_gain,
    )
    routed_out = routed_half(
        second_micro_tokens,
        expert_norm_gain,
        routes,
        visit_weight,
        gate_weight_table,
        up_weight_table,
        down_weight_table,
    )
    return (mixer_gated_output, routed_out)


def solution(mesh):
    torus = Mesh(mesh.devices.reshape(8, 4, 2, mesh.shape["tp"]), ("ep_0", "ep_1", "ep_2", "tp"))
    in_specs = (
        P(EP, "tp"),
        P(None, EP, "tp"),
        P(EP, "tp"),
        P(EP, "tp"),
        P("tp"),
        P("tp"),
        P(EP, "tp"),
        P("tp"),
        P(None, "tp"),
        P(None, None, "tp"),
        P("tp"),
        P(EP_TP, None),
        P(),
        P(EP_TP, None),
        P(EP_TP, None),
        P(EP, None, "tp"),
        P(EP, None, "tp"),
        P(EP, None, "tp"),
    )
    out_specs = (P(EP, "tp"), P(EP_TP, None))
    return jax.shard_map(body, mesh=torus, in_specs=in_specs, out_specs=out_specs, check_vma=False)
```

profile of v0, /device:TPU:1, one launch (start us, length us, event | category | flops | bytes accessed | tf_op | source)
XLA Modules:
  0.0 375.9 jit_solution(12267511515905905539)
XLA Ops:
  9.6 4.5 %collective-permute-start = (bf16[3,1024]{0,1:T(8,128)(2,1)}, bf16[3,1024]{0,1:T(8,128)(2,1)}, u32[]{:S(2)}, u32[]{:S(2)}) collective-permute-start(bf16[3,1024]{0,1:T(8,128)(2,1)} %copy.59), channel_id=1, source_target_pairs={{0,4},{4,8},{8,12},{12,16},{16,20},{20,24},{24,28},{28,32},{32,36}... | collective-permute-start | bytes 18440 | tf_op jit(solution)/shard_map/ppermute | solution.py:23
  14.0 2.2 slice_bitcast_fusion.1
  16.9 47.4 %fusion.58 = f32[8,128,2,4]{3,0,1,2:T(8,128)S(1)} fusion(f32[8,128,2,4]{3,0,1,2:T(8,128)S(1)} %copy.65), kind=kOutput, calls=%fused_computation.142 | output fusion | flops 1040384 | bytes 65536 | tf_op jit(solution)/shard_map/jit(cumsum)/reduce_window_sum | solution.py:105
  66.5 2.2 all-gather.3
  68.6 7.7 %all-gather.4 = f32[4,2,4]{2,1,0:T(2,128)S(1)} all-gather(f32[1,2,4]{2,1,0:T(2,128)S(1)} %fusion.54), channel_id=4, replica_groups=mesh['ep_0'=8,'ep_1'=4,'ep_2'=2,'tp'=4] {'ep_1'}, dimensions={0}, use_global_device_ids=true | all-gather | bytes 160 | tf_op jit(solution)/shard_map/all_gather | solution.py:37
  76.8 1.5 copy.60
  80.4 2.2 multiply_bitcast_fusion
  85.7 1.4 divide_multiply_fusion
  87.1 2.0 reshape.211
  90.5 1.8 fusion.16
  92.2 14.4 %while.13 = (s32[]{:T(128)}, f32[2,4,64,128]{3,2,1,0:T(8,128)S(1)}, f32[8,2,4,64,128]{4,3,2,1,0:T(8,128)}, f32[8,2,4]{2,1,0:T(2,128)S(1)}, f32[8,2,4,64,128]{4,3,2,1,0:T(8,128)}, /*index=5*/s32[]{:T(128)}, s32[]{:T(128)}) while((s32[]{:T(128)}, f32[2,4,64,128]{3,2,1,0:T(8,128)S(1)}, f32[8,2,4,64,128]{4,3,2,1,0:T(8,128)}, ...), condition=%wide.region_2.3_spmd.clone, body=%wide.region_1.2_spmd.clone.sunk | while | flops 262147 | bytes 1310924 | solution.py:119
  106.6 4.0 %all-gather.1 = f32[4,4,64,128]{3,2,1,0:T(8,128)S(1)} all-gather(f32[2,4,64,128]{3,2,1,0:T(8,128)S(1)} %get-tuple-element.31), channel_id=3, replica_groups=mesh['ep_0'=8,'ep_1'=4,'ep_2'=2,'tp'=4] {'ep_2'}, dimensions={0}, use_global_device_ids=true | all-gather | bytes 786432 | tf_op jit(solution)/shard_map/all_gather | solution.py:37
  112.5 24.1 %all-gather.8.cloned.1.call-done = f32[4,2,4,64,128]{4,3,2,1,0:T(8,128)} async-done(((f32[1,2,4,64,128]{4,3,2,1,0:T(8,128)}), f32[4,2,4,64,128]{4,3,2,1,0:T(8,128)}) %all-gather.8.cloned.1.call-update) | async-done | bytes 1048592 | tf_op jit(solution)/shard_map/all_gather | solution.py:37
  136.5 2.0 slice_add_fusion.8
  138.6 2.3 copy.80
  140.9 1.5 copy.66
  142.5 1.6 copy.77
  146.2 192.4 %shard_map.185 = bf16[256,2048]{1,0:T(8,128)(2,1)} custom-call(bf16[256,2048]{1,0:T(8,128)(2,1)} %tokens_hbm.1, f32[1,2048]{1,0:T(1,128)} %bitcast.195, s32[256,2]{1,0:T(8,128)} %copy.81.routes_ref, f32[256,2]{1,0:T(8,128)} %copy.82.weight_ref, bf16[1,2048,256]{2,1,0:T(8,128)(2,1)} %gate_hbm.1, bf16[1,2048,256]{2,1,0:T(8,128)(2,1)} %up_hbm.1, ...), custom_call_target="tpu_custom_call" | custom-call | flops 10000000000 | bytes 20000000 | tf_op jit(solution)/shard_map/pallas_call | solution.py:463
  338.6 12.5 %all_gather.28 = f32[8,2,4]{2,1,0:T(2,128)S(1)} all-gather(f32[1,2,4]{2,1,0:T(2,128)S(1)} %get-tuple-element.103), channel_id=1, replica_groups=mesh['ep_0'=8,'ep_1'=4,'ep_2'=2,'tp'=4] {'ep_0'}, dimensions={0}, use_global_device_ids=true | all-gather | bytes 288 | tf_op jit(solution)/shard_map/all_gather | solution.py:37
  351.1 1.4 divide_multiply_fusion.1
  353.7 1.6 fusion.37
  355.3 3.3 fusion
  358.7 2.5 fusion.45
  361.2 2.7 fusion.15
  (132 shorter events, 36.5 us)
Async XLA Ops:
  7.2 9.1 %copy-start.25 = (f32[8]{0:T(128)S(1)}, f32[8]{0:T(128)}, u32[]{:S(2)}) copy-start(f32[8]{0:T(128)} %param.25) | copy-start | bytes 100
  7.2 9.1 %copy-start.8 = (f32[1024,8]{0,1:T(8,128)S(1)}, f32[1024,8]{0,1:T(8,128)}, u32[]{:S(2)}) copy-start(f32[1024,8]{0,1:T(8,128)} %param.23) | copy-start | bytes 98308
  7.2 9.1 %copy-start.24 = (f32[8]{0:T(128)S(1)}, f32[8]{0:T(128)}, u32[]{:S(2)}) copy-start(f32[8]{0:T(128)} %param.24) | copy-start | bytes 100
  7.2 9.1 %copy-start.9 = (f32[1024,8]{0,1:T(8,128)S(1)}, f32[1024,8]{0,1:T(8,128)}, u32[]{:S(2)}) copy-start(f32[1024,8]{0,1:T(8,128)} %param.26) | copy-start | bytes 98308
  7.2 129.3 %all-gather.8.cloned.1.call-start = ((), (), s32[]{:S(2)}) async-start(), calls=%async_computation | async-start | bytes 1310720 | tf_op jit(solution)/shard_map/all_gather | solution.py:37
  9.6 69.3 %collective-permute-start = (bf16[3,1024]{0,1:T(8,128)(2,1)}, bf16[3,1024]{0,1:T(8,128)(2,1)}, u32[]{:S(2)}, u32[]{:S(2)}) collective-permute-start(bf16[3,1024]{0,1:T(8,128)(2,1)} %copy.59), channel_id=1, source_target_pairs={{0,4},{4,8},{8,12},{12,16},{16,20},{20,24},{24,28},{28,32},{32,36}... | collective-permute-start | bytes 18440 | tf_op jit(solution)/shard_map/ppermute | solution.py:23
  64.3 14.0 %copy-start = (f32[8,128,2,4]{3,0,1,2:T(8,128)}, f32[8,128,2,4]{3,0,1,2:T(8,128)S(1)}, u32[]{:S(2)}) copy-start(f32[8,128,2,4]{3,0,1,2:T(8,128)S(1)} %fusion.58) | copy-start | bytes 98308
  64.3 1.5 copy-start.11
  83.1 2.6 copy-start.17
  83.1 2.6 copy-start.18
  83.1 2.6 copy-start.19
  83.1 2.6 copy-start.20
  112.2 246.4 %all-gather.10.cloned.1.call-start = ((), (), s32[]{:S(2)}) async-start(), calls=%async_computation.1 | async-start | bytes 2359296 | tf_op jit(solution)/shard_map/all_gather | solution.py:37
  136.5 5.9 %copy-start.26 = (f32[8]{0:T(128)S(1)}, f32[8]{0:T(128)}, u32[]{:S(2)}) copy-start(f32[8]{0:T(128)} %param.27) | copy-start | bytes 100
  138.6 6.0 %copy-start.21 = (s32[256,2]{0,1:T(2,128)S(1)}, s32[256,2]{0,1:T(2,128)}, u32[]{:S(2)}) copy-start(s32[256,2]{0,1:T(2,128)} %param.33) | copy-start | bytes 6148
  138.6 6.8 %copy-start.22 = (f32[256,2]{0,1:T(2,128)S(1)}, f32[256,2]{0,1:T(2,128)}, u32[]{:S(2)}) copy-start(f32[256,2]{0,1:T(2,128)} %param.34) | copy-start | bytes 6148
  146.2 204.9 %copy-start.13 = (f32[1,1,256]{2,1,0:T(1,128)S(1)}, f32[1,1,256]{2,1,0:T(1,128)}, u32[]{:S(2)}) copy-start(f32[1,1,256]{2,1,0:T(1,128)} %get-tuple-element.108) | copy-start | bytes 3076
  146.2 204.9 %copy-start.14 = (f32[1,1,256]{2,1,0:T(1,128)S(1)}, f32[1,1,256]{2,1,0:T(1,128)}, u32[]{:S(2)}) copy-start(f32[1,1,256]{2,1,0:T(1,128)} %get-tuple-element.111) | copy-start | bytes 3076
  146.2 204.9 %copy-start.15 = (f32[1,1,256]{2,1,0:T(1,128)S(1)}, f32[1,1,256]{2,1,0:T(1,128)}, u32[]{:S(2)}) copy-start(f32[1,1,256]{2,1,0:T(1,128)} %get-tuple-element.112) | copy-start | bytes 3076
  146.2 204.9 %copy-start.16 = (f32[1,1,256]{2,1,0:T(1,128)S(1)}, f32[1,1,256]{2,1,0:T(1,128)}, u32[]{:S(2)}) copy-start(f32[1,1,256]{2,1,0:T(1,128)} %get-tuple-element.113) | copy-start | bytes 3076
  353.7 1.6 copy-start.7
  355.3 3.3 copy-start.3
  355.3 3.3 copy-start.12
  358.6 2.5 copy-start.5
  (6 other events, 7.1 us)
Sparse Core Ops, SparseCore 0:
  112.4 24.1 all-gather.7
  138.7 63.5 all-gather.9
where the time goes:
time: 379 us; the launch traced here: 376 us
  Pallas kernels  192 us (51%)
  other arithmetic  80 us (21%)
  blocking collectives  26.3 us (7%)
  local copies, waits for them, and re-layouts  24.3 us (6%)
  waiting for transfers between devices  24.1 us (6%)
  between operations  14.6 us (4%)
  matrix products  9.39 us (2%)
  starting transfers between devices  4.75 us (1%)
    pallas_call x1, Pallas kernels, routed_half(): pl.pallas_call(routed_kernel, out_shape=jax.ShapeDtypeStruct((256, 2048),...  192 us
    another operation x1, other arithmetic, mixer_half(): jnp.cumsum(decay_logarithm.reshape(blocks, BLOCK, groups, per_group), axi...  47.4 us
    all_gather x4, blocking collectives, entering_2(): pieces = jax.tree.map(lambda part: lax.all_gather(part, axis), total)  26.3 us
    all_gather x2, waiting for transfers between devices, entering_2(): pieces = jax.tree.map(lambda part: lax.all_gather(part, axis), total)  24.1 us
    unnamed x65, local copies, waits for them, and re-layouts  9.19 us
    add x8, other arithmetic, carry_block(): carry_state * jnp.exp(inputs[1])[..., None, None] + inputs[0]  8.36 us
  transfers between devices with their start and end apart: 3, of which 1 were waited for; matrix products, arithmetic and copies ran while one was open for 19% of the time, Pallas kernels for 51%

commit v1 on v0

v1 whole, which is shorter than its diff:
```python
import types

import jax
import jax.numpy as jnp
from jax import lax
from jax.experimental import pallas as pl
from jax.experimental.pallas import tpu as pltpu
from jax.sharding import Mesh
from jax.sharding import PartitionSpec as P

HEADDIM = 64
NSTATE = 128
BLOCK = 128
SEQ_BLOCKS = 8
EP = ("ep_0", "ep_1", "ep_2")
EP_TP = ("ep_0", "ep_1", "ep_2", "tp")


EPSILON = 1e-05
CONTRACT_LAST = (((1,), (1,)), ((), ()))


SLOTS = 12
ORDER = (4, 1, 7, 3, 5, 2, 6, 0)
MESH_IDS = pl.DeviceIdType.MESH


def here():
    return (lax.axis_index("ep_0"), lax.axis_index("ep_1"), lax.axis_index("ep_2"))


def beside(step):
    return {"tp": lax.rem(lax.axis_index("tp") + step, 4)}


def ep_target(place, dz, dxc):
    z, x, c = place
    tz = lax.rem(z + dz, 8)
    tx = lax.rem(x + lax.div(dxc, 2), 4)
    tc = lax.rem(c + lax.rem(dxc, 2), 2)
    return tz * 8 + tx * 2 + tc, {"ep_0": tz, "ep_1": tx, "ep_2": tc}


def for_all_peers(act):
    place = here()

    def some(dxc, unused):
        for dz in ORDER:
            act(*ep_target(place, dz, dxc))
        return unused

    for dz in ORDER:
        if dz:
            act(*ep_target(place, dz, 0))
    lax.fori_loop(1, 8, some, 0)


def exchange(source, landing, send_sem, recv_sem):
    z, x, c = here()
    me = z * 8 + x * 2 + c

    def send(index, device):
        pltpu.make_async_remote_copy(
            src_ref=source.at[index],
            dst_ref=landing.at[me],
            send_sem=send_sem,
            recv_sem=recv_sem,
            device_id=device,
            device_id_type=MESH_IDS,
        ).start()

    for_all_peers(send)


def all_but_one(source, landing, send_sem, recv_sem):
    return pltpu.make_async_remote_copy(
        src_ref=source.at[pl.ds(0, 63)],
        dst_ref=landing.at[pl.ds(0, 63)],
        send_sem=send_sem,
        recv_sem=recv_sem,
        device_id=beside(1),
        device_id_type=MESH_IDS,
    )


def floor_div(values, divisor):
    return jnp.floor((values + 0.5) * (1.0 / divisor))


def iota(shape, axis):
    return lax.broadcasted_iota(jnp.int32, shape, axis).astype(jnp.float32)


def dot(a, b):
    return jnp.dot(a, b, preferred_element_type=jnp.float32)


def repack_matrix():
    size = 16 * SLOTS
    row = iota((size, size), 0)
    outer = floor_div(row, 4 * SLOTS)
    rest = row - 4 * SLOTS * outer
    inner = floor_div(rest, SLOTS)
    partner = inner * (4 * SLOTS) + outer * SLOTS + (rest - inner * SLOTS)
    return jnp.where(iota((size, size), 1) == partner, 1.0, 0.0).astype(jnp.bfloat16)


def pack_rows(source, landing, matrix, width):
    def group(g, unused):
        rows = source[pl.ds(pl.multiple_of(g * 48, 16), 48), :]
        tall = jnp.concatenate([rows[:, p * width : (p + 1) * width] for p in range(4)], axis=0)
        landing[pl.ds(g * 4, 4)] = dot(matrix, tall).astype(jnp.bfloat16).reshape(4, 48, width)
        return unused

    lax.fori_loop(0, 16, group, 0)


def unpack_rows(source, landing, matrix, width):
    def group(g, unused):
        tall = source[pl.ds(g * 4, 4)].reshape(192, width)
        rows = dot(matrix, tall).astype(jnp.bfloat16)
        for p in range(4):
            landing[pl.ds(pl.multiple_of(g * 48, 16), 48), p * width : (p + 1) * width] = rows[
                p * 48 : (p + 1) * 48
            ]
        return unused

    lax.fori_loop(0, 16, group, 0)


class Neighbours:
    def __init__(self, own, slots, send_sems, recv_sems, first, start, size):
        half = size // 2
        whole, low, high = pl.ds(start, size), pl.ds(start, half), pl.ds(start + half, half)

        def copy(which, source, landing, step):
            return pltpu.make_async_remote_copy(
                src_ref=source,
                dst_ref=landing,
                send_sem=send_sems.at[first + which],
                recv_sem=recv_sems.at[first + which],
                device_id=beside(step),
                device_id_type=MESH_IDS,
            )

        self.near = (
            copy(0, own.at[0, whole], slots.at[1, whole], 1),
            copy(1, own.at[0, whole], slots.at[2, whole], 3),
        )
        self.far = (
            copy(2, slots.at[1, low], slots.at[3, low], 1),
            copy(3, slots.at[2, high], slots.at[3, high], 3),
        )

    def start(self):
        for copy in self.near:
            copy.start()

    def forward(self):
        for arrived, onward in zip(self.near, self.far):
            arrived.wait_recv()
            onward.start()

    def arrive(self):
        for copy in self.far:
            copy.wait_recv()

    def drain(self):
        for copy in self.near + self.far:
            copy.wait_send()


def exact_dot(a, b):
    return jnp.dot(a, b, precision=lax.Precision.HIGHEST, preferred_element_type=jnp.float32)


def softplus(values):
    small = jnp.exp(-jnp.abs(values))
    ratio = small / (2.0 + small)
    square = ratio * ratio
    series = 1.0 / 13.0
    for odd in (11.0, 9.0, 7.0, 5.0, 3.0, 1.0):
        series = series * square + 1.0 / odd
    return jnp.maximum(values, 0.0) + 2.0 * ratio * series


def head_spread(rows):
    return jnp.where(floor_div(iota((rows, 512), 1), HEADDIM) == iota((rows, 512), 0), 1.0, 0.0)


def conv_silu(window, taps):
    window = window.astype(jnp.float32)
    total = taps[3:4] * window[16:]
    for j in range(3):
        total = total + taps[j : j + 1] * pltpu.roll(window, 3 - j, 0)[16:]
    return jax.nn.silu(total)


def mixer_local(m):
    spread = head_spread(8)
    low = iota((BLOCK, BLOCK), 0)
    high = iota((BLOCK, BLOCK), 1)
    causal = low >= high
    lower = jnp.where(causal, 1.0, 0.0)
    first = iota((BLOCK, 512), 1)
    first = first - 128 * floor_div(first, 128) < 64
    gain = exact_dot(jnp.broadcast_to(m.direct_gain[...], (8, 8)), spread)[0:1]
    rate = -jnp.exp(m.log_decay[...])
    value_taps = m.value_taps[...].astype(jnp.float32)
    map_taps = m.map_taps[...].astype(jnp.float32)
    m.state[...] = jnp.zeros_like(m.state)

    def block(b, prefix):
        start = pl.multiple_of(b * BLOCK, BLOCK)
        rows, window = pl.ds(start, BLOCK), pl.ds(start, BLOCK + 16)
        x = conv_silu(m.values[window, :], value_taps)
        in_maps = conv_silu(m.maps[0, window, :], map_taps[0])
        out_maps = conv_silu(m.maps[1, window, :], map_taps[1]).astype(jnp.bfloat16)
        m.out_maps[rows, :] = out_maps
        step = softplus(m.step[rows, :] + m.step_bias[...])
        running = exact_dot(lower, rate * step + m.increment[rows, :])
        running_rows = jnp.transpose(running)
        total = running[BLOCK - 1 : BLOCK, :]
        m.decay[rows, :] = jnp.exp(prefix + running)
        scaled = x * exact_dot(step, spread)
        to_end = (x * exact_dot(step * jnp.exp(total - running), spread)).astype(jnp.bfloat16)
        entered = exact_dot(jnp.exp(running), spread)
        left = jnp.where(first, scaled, 0.0).astype(jnp.bfloat16)
        right = jnp.where(first, 0.0, scaled).astype(jnp.bfloat16)
        for g in range(2):
            maps = slice(g * NSTATE, (g + 1) * NSTATE)
            wide = slice(g * 256, (g + 1) * 256)
            scores = lax.dot_general(
                out_maps[:, maps],
                in_maps[:, maps].astype(jnp.bfloat16),
                CONTRACT_LAST,
                preferred_element_type=jnp.float32,
            )
            carried = dot(out_maps[:, maps], m.state[:, wide].astype(jnp.bfloat16))
            for pair in range(2):
                mixes = []
                for h in (g * 4 + 2 * pair, g * 4 + 2 * pair + 1):
                    ahead = running[:, h : h + 1] - running_rows[h : h + 1, :]
                    between = jnp.exp(jnp.where(causal, ahead, -jnp.inf))
                    mixes.append((scores * between).astype(jnp.bfloat16))
                part = slice((g * 2 + pair) * 128, (g * 2 + pair + 1) * 128)
                inside = dot(
                    jnp.concatenate(mixes, axis=1),
                    jnp.concatenate([left[:, part], right[:, part]], axis=0),
                )
                m.mixed[rows, part] = (
                    inside
                    + carried[:, pair * 128 : (pair + 1) * 128] * entered[:, part]
                    + x[:, part] * gain[:, part]
                )
            turned = jnp.transpose(in_maps[:, maps]).astype(jnp.bfloat16)
            m.state[:, wide] = m.state[:, wide] * entered[BLOCK - 1 : BLOCK, wide] + dot(
                turned, to_end[:, wide]
            )
        return prefix + total

    prefix = lax.fori_loop(0, SEQ_BLOCKS, block, jnp.zeros((1, 8), jnp.float32))
    for j in range(8):
        m.state_out[j] = m.state[j * 16 : (j + 1) * 16, :].astype(jnp.bfloat16)
    heads = jnp.where(iota((8, 128), 0) == iota((8, 128), 1), 1.0, 0.0)
    m.decay_out[...] = exact_dot(jnp.broadcast_to(jnp.exp(prefix), (8, 8)), heads)


def plane_target(dxc):
    z, x, c = here()
    tx = lax.rem(x + lax.div(dxc, 2), 4)
    tc = lax.rem(c + lax.rem(dxc, 2), 2)
    return tx * 2 + tc, {"ep_1": tx, "ep_2": tc}


def plane_send(source, landing, send_sem, recv_sem, indexed):
    z, x, c = here()
    mine = x * 2 + c

    def send(dxc, unused):
        index, device = plane_target(dxc)
        pltpu.make_async_remote_copy(
            src_ref=source.at[index] if indexed else source,
            dst_ref=landing.at[mine],
            send_sem=send_sem,
            recv_sem=recv_sem,
            device_id=device,
            device_id_type=MESH_IDS,
        ).start()
        return unused

    lax.fori_loop(1, 8, send, 0)


def plane_wait(landing, send_sem, recv_sem):
    pltpu.make_async_remote_copy(
        src_ref=landing.at[pl.ds(0, 7)],
        dst_ref=landing.at[pl.ds(0, 7)],
        send_sem=send_sem,
        recv_sem=recv_sem,
        device_id=beside(1),
        device_id_type=MESH_IDS,
    ).wait()


def later_copy(m, d, which):
    source, landing = ((m.plane_state, m.early_state), (m.plane_decay, m.early_decay))[which]
    return pltpu.make_async_remote_copy(
        src_ref=source,
        dst_ref=landing.at[d - 1],
        send_sem=m.later_send.at[which, d - 1],
        recv_sem=m.later_recv.at[which, d - 1],
        device_id={"ep_0": lax.rem(lax.axis_index("ep_0") + d, 8)},
        device_id_type=MESH_IDS,
    )


def states_first(m):
    z, x, c = here()
    mine = x * 2 + c
    m.plane_states[mine] = m.state_out[mine]
    m.plane_decays[mine] = m.decay_out[...]
    plane_send(m.state_out, m.plane_states, m.plane_sems.at[0], m.plane_sems.at[1], True)
    plane_send(m.decay_out, m.plane_decays, m.plane_sems.at[2], m.plane_sems.at[3], False)


def states_second(m):
    plane_wait(m.plane_states, m.plane_sems.at[0], m.plane_sems.at[1])
    plane_wait(m.plane_decays, m.plane_sems.at[2], m.plane_sems.at[3])
    spread = head_spread(128)
    before = jnp.zeros((16, 512), jnp.float32)
    passed = jnp.ones((8, 128), jnp.float32)
    for j in range(8):
        m.before[j] = before
        m.passed[j] = passed
        decay = m.plane_decays[j]
        before = before * exact_dot(decay, spread)[0:1] + m.plane_states[j].astype(jnp.float32)
        passed = passed * decay
    m.plane_state[...] = before.astype(jnp.bfloat16)
    m.plane_decay[...] = passed
    z = lax.axis_index("ep_0")
    for d in range(1, 8):

        @pl.when(z + d < 8)
        def _():
            for which in range(2):
                later_copy(m, d, which).start()


def states_third(m):
    z, x, c = here()
    spread = head_spread(128)
    m.incoming[...] = jnp.zeros_like(m.incoming)
    for d in range(7, 0, -1):

        @pl.when(z >= d)
        def _():
            for which in range(2):
                later_copy(m, d, which).wait_recv()
            m.incoming[...] = m.incoming[...] * exact_dot(m.early_decay[d - 1], spread)[
                0:1
            ] + m.early_state[d - 1].astype(jnp.float32)

    incoming = m.incoming[...]
    for j in range(8):
        entering = m.before[j] + exact_dot(m.passed[j], spread)[0:1] * incoming
        m.answer_states[j] = entering.astype(jnp.bfloat16)
    mine = x * 2 + c
    m.entering[mine] = m.answer_states[mine]
    plane_send(m.answer_states, m.entering, m.plane_sems.at[4], m.plane_sems.at[5], True)
    for d in range(1, 8):

        @pl.when(z + d < 8)
        def _():
            for which in range(2):
                later_copy(m, d, which).wait_send()


def mixer_finish(m):
    plane_wait(m.entering, m.plane_sems.at[4], m.plane_sems.at[5])
    spread = head_spread(8)
    entering = m.entering[...].reshape(128, 512)

    def block(b, unused):
        rows = pl.ds(pl.multiple_of(b * BLOCK, BLOCK), BLOCK)
        decay = exact_dot(m.decay[rows, :], spread)
        for g in range(2):
            wide = slice(g * 256, (g + 1) * 256)
            carried = dot(m.out_maps[rows, g * NSTATE : (g + 1) * NSTATE], entering[:, wide])
            gated = (m.mixed[rows, wide] + carried * decay[:, wide]) * jax.nn.silu(
                m.gate[rows, wide].astype(jnp.float32)
            )
            scale = lax.rsqrt(jnp.mean(gated * gated, axis=1, keepdims=True) + EPSILON)
            m.result[rows, wide] = (gated * scale * m.norm_gain[:, wide]).astype(jnp.bfloat16)
        return unused

    lax.fori_loop(0, SEQ_BLOCKS, block, 0)


BF16 = jnp.bfloat16
F32 = jnp.float32

INPUTS = (
    "tokens_hbm",
    "expert_gain",
    "routes",
    "visit_weight",
    "gate_hbm",
    "up_hbm",
    "down_hbm",
    "values_hbm",
    "maps_hbm",
    "gate_pre_hbm",
    "step_hbm",
    "increment_hbm",
    "step_bias",
    "log_decay",
    "direct_gain",
    "value_taps",
    "map_taps",
    "norm_gain",
)
OUTPUTS = ("result", "routed_out")
SCRATCH = dict(
    tokens=pltpu.VMEM((256, 2048), BF16),
    normed=pltpu.VMEM((256, 2048), BF16),
    choice=pltpu.VMEM((768, 256), BF16),
    mix_high=pltpu.VMEM((256, 768), BF16),
    mix_low=pltpu.VMEM((256, 768), BF16),
    rows=pltpu.VMEM((768, 2048), BF16),
    sent=pltpu.VMEM((64, 48, 512), BF16),
    landed=pltpu.VMEM((64, 48, 512), BF16),
    hidden=pltpu.VMEM((4, 768, 256), BF16),
    answers=pltpu.VMEM((4, 64, 48, 128), BF16),
    returned=pltpu.VMEM((4, 64, 48, 128), BF16),
    gate_slots=pltpu.VMEM((4, 2048, 256), BF16),
    up_slots=pltpu.VMEM((4, 2048, 256), BF16),
    down_slots=pltpu.VMEM((4, 2048, 256), BF16),
    values=pltpu.VMEM((1040, 512), BF16),
    maps=pltpu.VMEM((2, 1040, 256), BF16),
    gate=pltpu.VMEM((1024, 512), BF16),
    step=pltpu.VMEM((1024, 8), F32),
    increment=pltpu.VMEM((1024, 8), F32),
    decay=pltpu.VMEM((1024, 8), F32),
    mixed=pltpu.VMEM((1024, 512), F32),
    out_maps=pltpu.VMEM((1024, 256), BF16),
    state=pltpu.VMEM((128, 512), F32),
    state_out=pltpu.VMEM((8, 16, 512), BF16),
    decay_out=pltpu.VMEM((8, 128), F32),
    plane_states=pltpu.VMEM((8, 16, 512), BF16),
    plane_decays=pltpu.VMEM((8, 8, 128), F32),
    before=pltpu.VMEM((8, 16, 512), F32),
    passed=pltpu.VMEM((8, 8, 128), F32),
    plane_state=pltpu.VMEM((16, 512), BF16),
    plane_decay=pltpu.VMEM((8, 128), F32),
    early_state=pltpu.VMEM((7, 16, 512), BF16),
    early_decay=pltpu.VMEM((7, 8, 128), F32),
    incoming=pltpu.VMEM((16, 512), F32),
    answer_states=pltpu.VMEM((8, 16, 512), BF16),
    entering=pltpu.VMEM((8, 16, 512), BF16),
    local_sems=pltpu.SemaphoreType.DMA((9,)),
    near_send=pltpu.SemaphoreType.DMA((24,)),
    near_recv=pltpu.SemaphoreType.DMA((24,)),
    dispatch_sems=pltpu.SemaphoreType.DMA((2,)),
    answer_send=pltpu.SemaphoreType.DMA((4,)),
    answer_recv=pltpu.SemaphoreType.DMA((4,)),
    tail_send=pltpu.SemaphoreType.DMA((2,)),
    tail_recv=pltpu.SemaphoreType.DMA((2,)),
    plane_sems=pltpu.SemaphoreType.DMA((6,)),
    later_send=pltpu.SemaphoreType.DMA((2, 7)),
    later_recv=pltpu.SemaphoreType.DMA((2, 7)),
)


def kernel(*refs):
    m = types.SimpleNamespace(**dict(zip(INPUTS + OUTPUTS + tuple(SCRATCH), refs)))
    place = here()
    z, x, c = place
    me = z * 8 + x * 2 + c
    body = pl.ds(16, 1024)
    own_copies = [
        pltpu.make_async_copy(source, target, m.local_sems.at[i])
        for i, (source, target) in enumerate(
            (
                (m.tokens_hbm, m.tokens),
                (m.values_hbm, m.values.at[body]),
                (m.maps_hbm, m.maps.at[:, body]),
                (m.step_hbm, m.step),
                (m.increment_hbm, m.increment),
                (m.gate_pre_hbm, m.gate),
                (m.gate_hbm.at[0], m.gate_slots.at[0]),
                (m.up_hbm.at[0], m.up_slots.at[0]),
                (m.down_hbm.at[0], m.down_slots.at[0]),
            )
        )
    ]
    for copy in own_copies:
        copy.start()
    barrier = pltpu.get_barrier_semaphore()

    def greet(unused, device):
        pl.semaphore_signal(barrier, inc=1, device_id=device, device_id_type=MESH_IDS)

    for step in (1, 3):
        greet(0, beside(step))
    for_all_peers(greet)
    pl.semaphore_wait(barrier, 65)

    gate_near = Neighbours(m.gate_hbm, m.gate_slots, m.near_send, m.near_recv, 0, 0, 2048)
    up_near = Neighbours(m.up_hbm, m.up_slots, m.near_send, m.near_recv, 4, 0, 2048)
    down_near = [
        Neighbours(m.down_hbm, m.down_slots, m.near_send, m.near_recv, 8 + 4 * p, p * 512, 512)
        for p in range(4)
    ]
    gate_near.start()
    up_near.start()
    down_near[0].start()
    after = lax.rem(me + 1, 64)
    tails = [
        pltpu.make_async_remote_copy(
            src_ref=source,
            dst_ref=target,
            send_sem=m.tail_send.at[i],
            recv_sem=m.tail_recv.at[i],
            device_id={
                "ep_0": lax.div(after, 8),
                "ep_1": lax.rem(lax.div(after, 2), 4),
                "ep_2": lax.rem(after, 2),
            },
            device_id_type=MESH_IDS,
        )
        for i, (source, target) in enumerate(
            (
                (m.values_hbm.at[pl.ds(1008, 16)], m.values.at[pl.ds(0, 16)]),
                (m.maps_hbm.at[:, pl.ds(1008, 16)], m.maps.at[:, pl.ds(0, 16)]),
            )
        )
    ]
    for copy in tails:
        copy.start()

    own_copies[0].wait()

    def norm_rows(i, unused):
        rows = pl.ds(pl.multiple_of(i * 32, 32), 32)
        values = m.tokens[rows, :].astype(jnp.float32)
        centered = values - jnp.mean(values, axis=1, keepdims=True)
        scale = lax.rsqrt(jnp.mean(centered * centered, axis=1, keepdims=True) + EPSILON)
        m.normed[rows, :] = (centered * scale * m.expert_gain[...]).astype(jnp.bfloat16)
        return unused

    lax.fori_loop(0, 8, norm_rows, 0)

    experts = lax.broadcasted_iota(jnp.int32, (256, 64), 1)
    hits = [jnp.where(m.routes[:, k : k + 1] == experts, 1.0, 0.0) for k in range(2)]
    named = hits[0] + hits[1]
    earlier = jnp.where(iota((256, 256), 0) > iota((256, 256), 1), 1.0, 0.0).astype(jnp.bfloat16)
    slot = dot(earlier, named.astype(jnp.bfloat16))
    key = jnp.where(named > 0.5, slot, -1.0)
    key_rows = jnp.transpose(key).astype(jnp.bfloat16)
    spread = jnp.where(
        floor_div(iota((768, 64), 0), SLOTS) == iota((768, 64), 1), 1.0, 0.0
    ).astype(jnp.bfloat16)
    wanted = iota((768, 256), 0)
    wanted = wanted - SLOTS * floor_div(wanted, SLOTS)
    m.choice[...] = jnp.where(dot(spread, key_rows) == wanted, 1.0, 0.0).astype(jnp.bfloat16)
    matrix = repack_matrix()

    def pick(p, unused):
        columns = pl.ds(pl.multiple_of(p * 512, 512), 512)
        m.rows[:, columns] = dot(m.choice[...], m.normed[:, columns]).astype(jnp.bfloat16)
        return unused

    lax.fori_loop(0, 4, pick, 0)
    pack_rows(m.rows, m.sent, matrix, 512)
    exchange(m.sent, m.landed, m.dispatch_sems.at[0], m.dispatch_sems.at[1])
    m.landed[me] = m.sent[me]

    for copy in own_copies[1:5]:
        copy.wait()
    for copy in tails:
        copy.wait_recv()
    m.values[0:16, :] = jnp.where(me > 0, m.values[0:16, :], jnp.zeros((16, 512), jnp.bfloat16))
    m.maps[:, 0:16, :] = jnp.where(me > 0, m.maps[:, 0:16, :], jnp.zeros((2, 16, 256), jnp.bfloat16))
    mixer_local(m)
    gate_near.forward()
    states_first(m)

    weights = m.visit_weight[:, 0:1] * hits[0] + m.visit_weight[:, 1:2] * hits[1]
    spread_columns = jnp.where(
        floor_div(iota((64, 768), 1), SLOTS) == iota((64, 768), 0), 1.0, 0.0
    ).astype(jnp.bfloat16)
    wanted = iota((256, 768), 1)
    wanted = wanted - SLOTS * floor_div(wanted, SLOTS)
    mine = dot(key.astype(jnp.bfloat16), spread_columns) == wanted
    high = weights.astype(jnp.bfloat16)
    low = (weights - high.astype(jnp.float32)).astype(jnp.bfloat16)
    m.mix_high[...] = jnp.where(mine, dot(high, spread_columns), 0.0).astype(jnp.bfloat16)
    m.mix_low[...] = jnp.where(mine, dot(low, spread_columns), 0.0).astype(jnp.bfloat16)

    states_second(m)
    states_third(m)
    up_near.forward()
    down_near[0].forward()
    down_near[1].start()
    down_near[2].start()
    for copy in own_copies[5:]:
        copy.wait()
    mixer_finish(m)
    gate_near.arrive()
    up_near.arrive()

    all_but_one(m.sent, m.landed, m.dispatch_sems.at[0], m.dispatch_sems.at[1]).wait()
    unpack_rows(m.landed, m.rows, matrix, 512)

    def activate(j, unused):
        for r in range(3):
            rows = m.rows[r * 256 : (r + 1) * 256, :]
            opened = dot(rows, m.gate_slots[j])
            raised = dot(rows, m.up_slots[j])
            m.hidden[j, r * 256 : (r + 1) * 256, :] = (jax.nn.silu(opened) * raised).astype(
                jnp.bfloat16
            )
        return unused

    lax.fori_loop(0, 4, activate, 0)

    for p in range(4):
        down_near[p].arrive()

        def answer(n, unused):
            lines = pl.ds(pl.multiple_of(p * 512 + n * 256, 256), 256)
            total = jnp.zeros((768, 256), jnp.float32)
            for j in range(4):
                total = total + lax.dot_general(
                    m.hidden[j],
                    m.down_slots[j, lines, :],
                    CONTRACT_LAST,
                    preferred_element_type=jnp.float32,
                )
            m.rows[:, lines] = total.astype(jnp.bfloat16)
            return unused

        lax.fori_loop(0, 2, answer, 0)
        pack_rows(m.rows.at[:, pl.ds(p * 512, 512)], m.answers.at[p], matrix, 128)
        exchange(m.answers.at[p], m.returned.at[p], m.answer_send.at[p], m.answer_recv.at[p])
        m.returned[p, me] = m.answers[p, me]
        if p < 3:
            down_near[p + 1].forward()
        if p == 0:
            down_near[3].start()

    for p in range(4):
        all_but_one(
            m.answers.at[p], m.returned.at[p], m.answer_send.at[p], m.answer_recv.at[p]
        ).wait()
        lines = pl.ds(p * 512, 512)
        unpack_rows(m.returned.at[p], m.rows.at[:, lines], matrix, 128)
        m.routed_out[:, lines] = (
            dot(m.mix_high[...], m.rows[:, lines]) + dot(m.mix_low[...], m.rows[:, lines])
        ).astype(jnp.bfloat16)

    for near in [gate_near, up_near] + down_near:
        near.drain()
    for copy in tails:
        copy.wait_send()


def body(
    first_micro_values,
    group_state_maps,
    gate_preactivation,
    step_preactivation,
    head_step_bias,
    head_log_decay,
    decay_increment,
    head_direct_gain,
    convolution_value_taps,
    convolution_map_taps,
    grouped_norm_gain,
    second_micro_tokens,
    expert_norm_gain,
    routes,
    visit_weight,
    gate_weight_table,
    up_weight_table,
    down_weight_table,
):
    operands = (
        second_micro_tokens,
        expert_norm_gain.reshape(1, -1),
        routes,
        visit_weight,
        gate_weight_table,
        up_weight_table,
        down_weight_table,
        first_micro_values,
        group_state_maps,
        gate_preactivation,
        step_preactivation,
        decay_increment,
        head_step_bias.reshape(1, -1),
        head_log_decay.reshape(1, -1),
        head_direct_gain.reshape(1, -1),
        convolution_value_taps,
        convolution_map_taps,
        grouped_norm_gain.reshape(1, -1),
    )
    vmem = pl.BlockSpec(memory_space=pltpu.VMEM)
    hbm = pl.BlockSpec(memory_space=pl.ANY)
    return pl.pallas_call(
        kernel,
        out_shape=(
            jax.ShapeDtypeStruct((1024, 512), BF16),
            jax.ShapeDtypeStruct((256, 2048), BF16),
        ),
        in_specs=[hbm if name.endswith("_hbm") else vmem for name in INPUTS],
        out_specs=(vmem, vmem),
        scratch_shapes=list(SCRATCH.values()),
        compiler_params=pltpu.CompilerParams(
            collective_id=0, has_side_effects=True, vmem_limit_bytes=60 * 2**20
        ),
    )(*operands)


def solution(mesh):
    torus = Mesh(mesh.devices.reshape(8, 4, 2, mesh.shape["tp"]), ("ep_0", "ep_1", "ep_2", "tp"))
    in_specs = (
        P(EP, "tp"),
        P(None, EP, "tp"),
        P(EP, "tp"),
        P(EP, "tp"),
        P("tp"),
        P("tp"),
        P(EP, "tp"),
        P("tp"),
        P(None, "tp"),
        P(None, None, "tp"),
        P("tp"),
        P(EP_TP, None),
        P(),
        P(EP_TP, None),
        P(EP_TP, None),
        P(EP, None, "tp"),
        P(EP, None, "tp"),
        P(EP, None, "tp"),
    )
    out_specs = (P(EP, "tp"), P(EP_TP, None))
    return jax.shard_map(body, mesh=torus, in_specs=in_specs, out_specs=out_specs, check_vma=False)
```

time: 379 us -> 207 us (0.55)
  other arithmetic: 80 us -> 0 us
  blocking collectives: 26.3 us -> 0 us
  waiting for transfers between devices: 24.1 us -> 0 us
  local copies, waits for them, and re-layouts: 24.3 us -> 7.59 us
  between operations: 14.6 us -> 0.66 us
  matrix products: 9.39 us -> 0 us
  Pallas kernels: 192 us -> 199 us
  starting transfers between devices: 4.75 us -> 0 us
    another operation x3 -> x0, other arithmetic: 47.8 us -> none  [the longest x1 47.4 us: mixer_half(): jnp.cumsum(decay_logarithm.reshape(blocks, BLOCK, groups, per_group), axi...]
    all_gather x4 -> x0, blocking collectives: 26.3 us -> none  [entering_2(): pieces = jax.tree.map(lambda part: lax.all_gather(part, axis), total)]
    all_gather x2 -> x0, waiting for transfers between devices: 24.1 us -> none  [entering_2(): pieces = jax.tree.map(lambda part: lax.all_gather(part, axis), total)]
    add x10 -> x0, other arithmetic: 11.2 us -> none  [the longest x8 8.36 us: carry_block(): carry_state * jnp.exp(inputs[1])[..., None, None] + inputs[0]]
    dot_general x4 -> x0, matrix products: 9.39 us -> none  [the longest x1 3.29 us: mixer_half(): jnp.einsum('bgrls,bsgrp->blgrp', scores[:, :, None] * between, scaled_val...]
    pallas_call x1, Pallas kernels: 192 us -> 199 us  [body(): pl.pallas_call(kernel, out_shape=(jax.ShapeDtypeStruct((1024, 512), BF16)...]
    mul x6 -> x0, other arithmetic: 5.89 us -> none  [the longest x2 2.88 us: causal_conv(): return jax.nn.silu(summed_total)]
    dynamic_update_slice x8 -> x0, other arithmetic: 5.83 us -> none  [mixer_half(): lax.scan(carry_block, zero_state, (block_states, block_total))]
  transfers between devices with their start and end apart: 3 -> 0, of which waited for: 1 -> 0; matrix products, arithmetic and copies ran while one was open for 19% -> 0% of each run, Pallas kernels for 51% -> 0%
where the time goes in v1:
time: 207 us
  Pallas kernels  199 us (96%)
  local copies, waits for them, and re-layouts  7.59 us (4%)
    pallas_call x1, Pallas kernels, body(): pl.pallas_call(kernel, out_shape=(jax.ShapeDtypeStruct((1024, 512), BF16)...  199 us
    unnamed x16, local copies, waits for them, and re-layouts  7.59 us

profile of v1, /device:TPU:1, one launch (start us, length us, event | category | flops | bytes accessed | tf_op | source)
XLA Modules:
  0.0 207.3 jit_solution(6958513585868363329)
XLA Ops:
  0.6 0.0 copy-start.3
  0.6 0.7 copy-done.3
  1.3 0.0 copy-start.4
  1.3 0.8 copy.20.refs_2_
  2.1 0.0 copy-done.4
  2.1 0.0 copy-start.1
  2.1 0.8 copy.21.refs_3_
  2.9 0.0 copy-done.1
  2.9 0.0 copy-start.2
  2.9 1.0 copy.22.refs_10_
  3.9 0.0 copy-done.2
  3.9 1.0 copy.23.refs_11_
  4.9 199.0 %shard_map.185 = (bf16[1024,512]{1,0:T(8,128)(2,1)}, bf16[256,2048]{1,0:T(8,128)(2,1)}) custom-call(bf16[256,2048]{1,0:T(8,128)(2,1)} %refs_0_.1, f32[1,2048]{1,0:T(1,128)} %bitcast.5, s32[256,2]{1,0:T(8,128)} %copy.20.refs_2_, f32[256,2]{1,0:T(8,128)} %copy.21.refs_3_, bf16[1,2048,256]{2,1,0:T(8,128)(2,1)} %refs_4_.1, bf16[1,2048,256]{2,1,0:T(8,128)(2,1)} %refs_5_.1, ...), custom_call_target="tpu_custom_call" | custom-call | tf_op jit(solution)/shard_map/pallas_call | solution.py:711
  203.9 0.0 copy-start
  204.0 2.4 %copy.26 = bf16[1024,512]{1,0:T(8,128)(2,1)} copy(bf16[1024,512]{1,0:T(8,128)(2,1)} %get-tuple-element.4) | data formatting | bytes 2097152
  206.3 0.0 copy-done
  206.3 1.0 copy.27
Async XLA Ops:
  0.6 0.7 copy-start.3
  1.3 0.8 copy-start.4
  2.1 0.8 copy-start.1
  2.9 1.0 copy-start.2
  203.9 2.4 %copy-start = (bf16[256,2048]{1,0:T(8,128)(2,1)S(1)}, bf16[256,2048]{1,0:T(8,128)(2,1)}, u32[]{:S(2)}) copy-start(bf16[256,2048]{1,0:T(8,128)(2,1)} %get-tuple-element.5) | copy-start | bytes 3145732

commit v2 on v1

--- a/solution.py
+++ b/solution.py
@@ -33,49 +33,57 @@
     return {"tp": lax.rem(lax.axis_index("tp") + step, 4)}
 
 
-def ep_target(place, dz, dxc):
+def around(place, dz, dxc, sign):
     z, x, c = place
-    tz = lax.rem(z + dz, 8)
-    tx = lax.rem(x + lax.div(dxc, 2), 4)
-    tc = lax.rem(c + lax.rem(dxc, 2), 2)
-    return tz * 8 + tx * 2 + tc, {"ep_0": tz, "ep_1": tx, "ep_2": tc}
+    return {
+        "ep_0": lax.rem(z + (dz if sign > 0 else 8 - dz), 8),
+        "ep_1": lax.rem(x + (lax.div(dxc, 2) if sign > 0 else 4 - lax.div(dxc, 2)), 4),
+        "ep_2": lax.rem(c + lax.rem(dxc, 2), 2),
+    }
+
+
+def for_peers(dxc, act, sign):
+    place = here()
+    for i, dz in enumerate(ORDER):
+        act(i, around(place, dz, dxc, sign))
 
 
 def for_all_peers(act):
     place = here()
+    for i, dz in enumerate(ORDER[:7]):
+        act(i, around(place, dz, 0, 1))
 
     def some(dxc, unused):
-        for dz in ORDER:
-            act(*ep_target(place, dz, dxc))
+        for_peers(dxc, lambda i, device: act(dxc * 8 + i, device), 1)
         return unused
 
-    for dz in ORDER:
-        if dz:
-            act(*ep_target(place, dz, 0))
     lax.fori_loop(1, 8, some, 0)
 
 
-def exchange(source, landing, send_sem, recv_sem):
-    z, x, c = here()
-    me = z * 8 + x * 2 + c
-
-    def send(index, device):
-        pltpu.make_async_remote_copy(
-            src_ref=source.at[index],
-            dst_ref=landing.at[me],
-            send_sem=send_sem,
-            recv_sem=recv_sem,
-            device_id=device,
-            device_id_type=MESH_IDS,
-        ).start()
-
-    for_all_peers(send)
-
-
-def all_but_one(source, landing, send_sem, recv_sem):
+def row_copy(source, landing, index, send_sem, recv_sem, device):
     return pltpu.make_async_remote_copy(
-        src_ref=source.at[pl.ds(0, 63)],
-        dst_ref=landing.at[pl.ds(0, 63)],
+        src_ref=source.at[index],
+        dst_ref=landing.at[index],
+        send_sem=send_sem,
+        recv_sem=recv_sem,
+        device_id=device,
+        device_id_type=MESH_IDS,
+    )
+
+
+def send_group(source, landing, dxc, send_sem, recv_sem, sign):
+    place = here()
+    first = isinstance(dxc, int) and dxc == 0
+    for i, dz in enumerate(ORDER[:7] if first else ORDER):
+        device = around(place, dz, dxc, sign)
+        row_copy(source, landing, dxc * 8 + i, send_sem, recv_sem, device).start()
+
+
+def half_bytes(source, landing, half, send_sem, recv_sem):
+    rows = pl.ds(0, 31) if half == 0 else pl.ds(32, 32)
+    return pltpu.make_async_remote_copy(
+        src_ref=source.at[rows],
+        dst_ref=landing.at[rows],
         send_sem=send_sem,
         recv_sem=recv_sem,
         device_id=beside(1),
@@ -105,27 +113,18 @@
     return jnp.where(iota((size, size), 1) == partner, 1.0, 0.0).astype(jnp.bfloat16)
 
 
-def pack_rows(source, landing, matrix, width):
-    def group(g, unused):
-        rows = source[pl.ds(pl.multiple_of(g * 48, 16), 48), :]
-        tall = jnp.concatenate([rows[:, p * width : (p + 1) * width] for p in range(4)], axis=0)
-        landing[pl.ds(g * 4, 4)] = dot(matrix, tall).astype(jnp.bfloat16).reshape(4, 48, width)
-        return unused
-
-    lax.fori_loop(0, 16, group, 0)
-
-
-def unpack_rows(source, landing, matrix, width):
-    def group(g, unused):
-        tall = source[pl.ds(g * 4, 4)].reshape(192, width)
-        rows = dot(matrix, tall).astype(jnp.bfloat16)
+def pack_group(rows, matrix, width):
+    tall = jnp.concatenate([rows[:, p * width : (p + 1) * width] for p in range(4)], axis=0)
+    return dot(matrix, tall).astype(jnp.bfloat16).reshape(4, 48, width)
+
+
+def unpack_half(source, landing, matrix, half, column, width):
+    for g in range(half * 8, half * 8 + 8):
+        rows = dot(matrix, source[g * 4 : g * 4 + 4].reshape(192, width)).astype(jnp.bfloat16)
         for p in range(4):
-            landing[pl.ds(pl.multiple_of(g * 48, 16), 48), p * width : (p + 1) * width] = rows[
+            landing[g * 48 : (g + 1) * 48, column + p * width : column + (p + 1) * width] = rows[
                 p * 48 : (p + 1) * 48
             ]
-        return unused
-
-    lax.fori_loop(0, 16, group, 0)
 
 
 class Neighbours:
@@ -196,16 +195,21 @@
     return jax.nn.silu(total)
 
 
+def column_of(ref):
+    return jnp.transpose(jnp.broadcast_to(ref[...], (8, 8)))[:, 0:1]
+
+
 def mixer_local(m):
     spread = head_spread(8)
     low = iota((BLOCK, BLOCK), 0)
     high = iota((BLOCK, BLOCK), 1)
     causal = low >= high
-    lower = jnp.where(causal, 1.0, 0.0)
+    upper = jnp.where(low <= high, 1.0, 0.0)
     first = iota((BLOCK, 512), 1)
     first = first - 128 * floor_div(first, 128) < 64
     gain = exact_dot(jnp.broadcast_to(m.direct_gain[...], (8, 8)), spread)[0:1]
-    rate = -jnp.exp(m.log_decay[...])
+    rate = -jnp.exp(column_of(m.log_decay))
+    step_bias = column_of(m.step_bias)
     value_taps = m.value_taps[...].astype(jnp.float32)
     map_taps = m.map_taps[...].astype(jnp.float32)
     m.state[...] = jnp.zeros_like(m.state)
@@ -217,9 +221,10 @@
         in_maps = conv_silu(m.maps[0, window, :], map_taps[0])
         out_maps = conv_silu(m.maps[1, window, :], map_taps[1]).astype(jnp.bfloat16)
         m.out_maps[rows, :] = out_maps
-        step = softplus(m.step[rows, :] + m.step_bias[...])
-        running = exact_dot(lower, rate * step + m.increment[rows, :])
-        running_rows = jnp.transpose(running)
+        step_rows = softplus(m.step[:, rows] + step_bias)
+        running_rows = exact_dot(rate * step_rows + m.increment[:, rows], upper)
+        running = jnp.transpose(running_rows)
+        step = jnp.transpose(step_rows)
         total = running[BLOCK - 1 : BLOCK, :]
         m.decay[rows, :] = jnp.exp(prefix + running)
         scaled = x * exact_dot(step, spread)
@@ -431,16 +436,17 @@
     sent=pltpu.VMEM((64, 48, 512), BF16),
     landed=pltpu.VMEM((64, 48, 512), BF16),
     hidden=pltpu.VMEM((4, 768, 256), BF16),
-    answers=pltpu.VMEM((4, 64, 48, 128), BF16),
-    returned=pltpu.VMEM((4, 64, 48, 128), BF16),
+    answers=pltpu.VMEM((2, 64, 48, 256), BF16),
+    returned=pltpu.VMEM((2, 64, 48, 256), BF16),
+    total=pltpu.VMEM((256, 1024), F32),
     gate_slots=pltpu.VMEM((4, 2048, 256), BF16),
     up_slots=pltpu.VMEM((4, 2048, 256), BF16),
     down_slots=pltpu.VMEM((4, 2048, 256), BF16),
     values=pltpu.VMEM((1040, 512), BF16),
     maps=pltpu.VMEM((2, 1040, 256), BF16),
     gate=pltpu.VMEM((1024, 512), BF16),
-    step=pltpu.VMEM((1024, 8), F32),
-    increment=pltpu.VMEM((1024, 8), F32),
+    step=pltpu.VMEM((8, 1024), F32),
+    increment=pltpu.VMEM((8, 1024), F32),
     decay=pltpu.VMEM((1024, 8), F32),
     mixed=pltpu.VMEM((1024, 512), F32),
     out_maps=pltpu.VMEM((1024, 256), BF16),
@@ -461,7 +467,7 @@
     local_sems=pltpu.SemaphoreType.DMA((9,)),
     near_send=pltpu.SemaphoreType.DMA((24,)),
     near_recv=pltpu.SemaphoreType.DMA((24,)),
-    dispatch_sems=pltpu.SemaphoreType.DMA((2,)),
+    dispatch_sems=pltpu.SemaphoreType.DMA((4,)),
     answer_send=pltpu.SemaphoreType.DMA((4,)),
     answer_recv=pltpu.SemaphoreType.DMA((4,)),
     tail_send=pltpu.SemaphoreType.DMA((2,)),
@@ -504,6 +510,17 @@
     for step in (1, 3):
         greet(0, beside(step))
     for_all_peers(greet)
+    own_copies[0].wait()
+
+    def norm_rows(i, unused):
+        rows = pl.ds(pl.multiple_of(i * 32, 32), 32)
+        values = m.tokens[rows, :].astype(jnp.float32)
+        centered = values - jnp.mean(values, axis=1, keepdims=True)
+        scale = lax.rsqrt(jnp.mean(centered * centered, axis=1, keepdims=True) + EPSILON)
+        m.normed[rows, :] = (centered * scale * m.expert_gain[...]).astype(jnp.bfloat16)
+        return unused
+
+    lax.fori_loop(0, 8, norm_rows, 0)
     pl.semaphore_wait(barrier, 65)
 
     gate_near = Neighbours(m.gate_hbm, m.gate_slots, m.near_send, m.near_recv, 0, 0, 2048)
@@ -514,7 +531,6 @@
     ]
     gate_near.start()
     up_near.start()
-    down_near[0].start()
     after = lax.rem(me + 1, 64)
     tails = [
         pltpu.make_async_remote_copy(
@@ -539,31 +555,36 @@
     for copy in tails:
         copy.start()
 
-    own_copies[0].wait()
-
-    def norm_rows(i, unused):
-        rows = pl.ds(pl.multiple_of(i * 32, 32), 32)
-        values = m.tokens[rows, :].astype(jnp.float32)
-        centered = values - jnp.mean(values, axis=1, keepdims=True)
-        scale = lax.rsqrt(jnp.mean(centered * centered, axis=1, keepdims=True) + EPSILON)
-        m.normed[rows, :] = (centered * scale * m.expert_gain[...]).astype(jnp.bfloat16)
-        return unused
-
-    lax.fori_loop(0, 8, norm_rows, 0)
-
-    experts = lax.broadcasted_iota(jnp.int32, (256, 64), 1)
-    hits = [jnp.where(m.routes[:, k : k + 1] == experts, 1.0, 0.0) for k in range(2)]
+    experts = lax.broadcasted_iota(jnp.int32, (64, 256), 0)
+    hits = [jnp.where(m.routes[k : k + 1, :] == experts, 1.0, 0.0) for k in range(2)]
     named = hits[0] + hits[1]
-    earlier = jnp.where(iota((256, 256), 0) > iota((256, 256), 1), 1.0, 0.0).astype(jnp.bfloat16)
-    slot = dot(earlier, named.astype(jnp.bfloat16))
+    earlier = jnp.where(iota((256, 256), 0) < iota((256, 256), 1), 1.0, 0.0).astype(jnp.bfloat16)
+    slot = dot(named.astype(jnp.bfloat16), earlier)
     key = jnp.where(named > 0.5, slot, -1.0)
-    key_rows = jnp.transpose(key).astype(jnp.bfloat16)
+    peer = iota((64, 64), 0)
+    plane = floor_div(peer, 8)
+    turn = peer - 8.0 * plane
+    ahead = jnp.zeros((64, 64), jnp.float32)
+    for i, dz in enumerate(ORDER):
+        ahead = ahead + jnp.where(turn == float(i), float(dz), 0.0)
+    plane_x = floor_div(plane, 2)
+    to_z = ahead + z.astype(jnp.float32)
+    to_x = plane_x + x.astype(jnp.float32)
+    to_c = plane - 2.0 * plane_x + c.astype(jnp.float32)
+    to_z = to_z - 8.0 * floor_div(to_z, 8)
+    to_x = to_x - 4.0 * floor_div(to_x, 4)
+    to_c = to_c - 2.0 * floor_div(to_c, 2)
+    expert_of = jnp.where(to_z * 8.0 + to_x * 2.0 + to_c == iota((64, 64), 1), 1.0, 0.0)
+    expert_of = expert_of.astype(jnp.bfloat16)
+    key = dot(expert_of, key.astype(jnp.bfloat16))
     spread = jnp.where(
         floor_div(iota((768, 64), 0), SLOTS) == iota((768, 64), 1), 1.0, 0.0
     ).astype(jnp.bfloat16)
     wanted = iota((768, 256), 0)
     wanted = wanted - SLOTS * floor_div(wanted, SLOTS)
-    m.choice[...] = jnp.where(dot(spread, key_rows) == wanted, 1.0, 0.0).astype(jnp.bfloat16)
+    m.choice[...] = jnp.where(
+        dot(spread, key.astype(jnp.bfloat16)) == wanted, 1.0, 0.0
+    ).astype(jnp.bfloat16)
     matrix = repack_matrix()
 
     def pick(p, unused):
@@ -572,9 +593,33 @@
         return unused
 
     lax.fori_loop(0, 4, pick, 0)
-    pack_rows(m.rows, m.sent, matrix, 512)
-    exchange(m.sent, m.landed, m.dispatch_sems.at[0], m.dispatch_sems.at[1])
-    m.landed[me] = m.sent[me]
+
+    def pack_dispatch(dxc):
+        for g in range(2):
+            rows = m.rows[pl.ds(pl.multiple_of(dxc * 96 + g * 48, 16), 48), :]
+            m.sent[pl.ds(dxc * 8 + g * 4, 4)] = pack_group(rows, matrix, 512)
+
+    def send_dispatch(dxc, half):
+        send_group(m.sent, m.landed, dxc, m.dispatch_sems.at[half], m.dispatch_sems.at[2 + half], 1)
+
+    pack_dispatch(0)
+    pack_dispatch(1)
+    send_dispatch(0, 0)
+
+    def dispatch_first(dxc, unused):
+        pack_dispatch(dxc + 1)
+        send_dispatch(dxc, 0)
+        return unused
+
+    def dispatch_second(dxc, unused):
+        pack_dispatch(dxc + 1)
+        send_dispatch(dxc, 1)
+        return unused
+
+    lax.fori_loop(1, 4, dispatch_first, 0)
+    lax.fori_loop(4, 7, dispatch_second, 0)
+    m.landed[7] = m.sent[7]
+    send_dispatch(jnp.int32(7), 1)
 
     for copy in own_copies[1:5]:
         copy.wait()
@@ -583,82 +628,118 @@
     m.values[0:16, :] = jnp.where(me > 0, m.values[0:16, :], jnp.zeros((16, 512), jnp.bfloat16))
     m.maps[:, 0:16, :] = jnp.where(me > 0, m.maps[:, 0:16, :], jnp.zeros((2, 16, 256), jnp.bfloat16))
     mixer_local(m)
-    gate_near.forward()
     states_first(m)
 
-    weights = m.visit_weight[:, 0:1] * hits[0] + m.visit_weight[:, 1:2] * hits[1]
+    weights = m.visit_weight[0:1, :] * hits[0] + m.visit_weight[1:2, :] * hits[1]
     spread_columns = jnp.where(
         floor_div(iota((64, 768), 1), SLOTS) == iota((64, 768), 0), 1.0, 0.0
     ).astype(jnp.bfloat16)
     wanted = iota((256, 768), 1)
     wanted = wanted - SLOTS * floor_div(wanted, SLOTS)
-    mine = dot(key.astype(jnp.bfloat16), spread_columns) == wanted
+    mine = dot(jnp.transpose(key).astype(jnp.bfloat16), spread_columns) == wanted
     high = weights.astype(jnp.bfloat16)
     low = (weights - high.astype(jnp.float32)).astype(jnp.bfloat16)
-    m.mix_high[...] = jnp.where(mine, dot(high, spread_columns), 0.0).astype(jnp.bfloat16)
-    m.mix_low[...] = jnp.where(mine, dot(low, spread_columns), 0.0).astype(jnp.bfloat16)
-
-    states_second(m)
-    states_third(m)
-    up_near.forward()
-    down_near[0].forward()
-    down_near[1].start()
-    down_near[2].start()
+    for part, target in ((high, m.mix_high), (low, m.mix_low)):
+        turned = jnp.transpose(dot(expert_of, part)).astype(jnp.bfloat16)
+        target[...] = jnp.where(mine, dot(turned, spread_columns), 0.0).astype(jnp.bfloat16)
+
     for copy in own_copies[5:]:
         copy.wait()
-    mixer_finish(m)
+    gate_near.forward()
+    up_near.forward()
+    down_near[0].start()
+    down_near[1].start()
+    states_second(m)
     gate_near.arrive()
     up_near.arrive()
 
-    all_but_one(m.sent, m.landed, m.dispatch_sems.at[0], m.dispatch_sems.at[1]).wait()
-    unpack_rows(m.landed, m.rows, matrix, 512)
-
-    def activate(j, unused):
-        for r in range(3):
-            rows = m.rows[r * 256 : (r + 1) * 256, :]
+    def activate(half):
+        half_bytes(m.sent, m.landed, half, m.dispatch_sems.at[half], m.dispatch_sems.at[2 + half]).wait()
+        unpack_half(m.landed, m.rows, matrix, half, 0, 512)
+
+        def one(j, unused):
+            rows = m.rows[half * 384 : (half + 1) * 384, :]
             opened = dot(rows, m.gate_slots[j])
             raised = dot(rows, m.up_slots[j])
-            m.hidden[j, r * 256 : (r + 1) * 256, :] = (jax.nn.silu(opened) * raised).astype(
+            m.hidden[j, half * 384 : (half + 1) * 384, :] = (jax.nn.silu(opened) * raised).astype(
                 jnp.bfloat16
             )
-        return unused
-
-    lax.fori_loop(0, 4, activate, 0)
-
-    for p in range(4):
-        down_near[p].arrive()
-
-        def answer(n, unused):
-            lines = pl.ds(pl.multiple_of(p * 512 + n * 256, 256), 256)
-            total = jnp.zeros((768, 256), jnp.float32)
+            return unused
+
+        lax.fori_loop(0, 4, one, 0)
+
+    def answer(half, p):
+        inside = slice(half * 384, (half + 1) * 384)
+
+        def one(n, unused):
+            lines = pl.ds(pl.multiple_of(p * 1024 + n * 256, 256), 256)
+            total = jnp.zeros((384, 256), jnp.float32)
             for j in range(4):
                 total = total + lax.dot_general(
-                    m.hidden[j],
+                    m.hidden[j, inside],
                     m.down_slots[j, lines, :],
                     CONTRACT_LAST,
                     preferred_element_type=jnp.float32,
                 )
-            m.rows[:, lines] = total.astype(jnp.bfloat16)
+            m.rows[inside, lines] = total.astype(jnp.bfloat16)
             return unused
 
-        lax.fori_loop(0, 2, answer, 0)
-        pack_rows(m.rows.at[:, pl.ds(p * 512, 512)], m.answers.at[p], matrix, 128)
-        exchange(m.answers.at[p], m.returned.at[p], m.answer_send.at[p], m.answer_recv.at[p])
-        m.returned[p, me] = m.answers[p, me]
-        if p < 3:
-            down_near[p + 1].forward()
-        if p == 0:
-            down_near[3].start()
-
-    for p in range(4):
-        all_but_one(
-            m.answers.at[p], m.returned.at[p], m.answer_send.at[p], m.answer_recv.at[p]
-        ).wait()
-        lines = pl.ds(p * 512, 512)
-        unpack_rows(m.returned.at[p], m.rows.at[:, lines], matrix, 128)
-        m.routed_out[:, lines] = (
-            dot(m.mix_high[...], m.rows[:, lines]) + dot(m.mix_low[...], m.rows[:, lines])
-        ).astype(jnp.bfloat16)
+        lax.fori_loop(0, 4, one, 0)
+        for g in range(half * 8, half * 8 + 8):
+            m.answers[p, g * 4 : g * 4 + 4] = pack_group(
+                m.rows[g * 48 : (g + 1) * 48, p * 1024 : (p + 1) * 1024], matrix, 256
+            )
+        which = 2 * p + half
+        sems = (m.answer_send.at[which], m.answer_recv.at[which])
+        if half == 0:
+            m.returned[p, 7] = m.answers[p, 7]
+            send_group(m.answers.at[p], m.returned.at[p], 0, *sems, -1)
+
+        def some(dxc, unused):
+            send_group(m.answers.at[p], m.returned.at[p], dxc, *sems, -1)
+            return unused
+
+        lax.fori_loop(max(1, half * 4), half * 4 + 4, some, 0)
+
+    activate(0)
+    down_near[0].forward()
+    down_near[1].forward()
+    down_near[2].start()
+    down_near[3].start()
+    activate(1)
+    states_third(m)
+    down_near[0].arrive()
+    down_near[1].arrive()
+    answer(0, 0)
+    answer(1, 0)
+    down_near[2].forward()
+    down_near[3].forward()
+    down_near[2].arrive()
+    down_near[3].arrive()
+    answer(0, 1)
+    answer(1, 1)
+    mixer_finish(m)
+
+    for p in range(2):
+        lines = pl.ds(p * 1024, 1024)
+        for half in range(2):
+            which = 2 * p + half
+            half_bytes(
+                m.answers.at[p],
+                m.returned.at[p],
+                half,
+                m.answer_send.at[which],
+                m.answer_recv.at[which],
+            ).wait()
+            unpack_half(m.returned.at[p], m.rows, matrix, half, p * 1024, 256)
+            inside = slice(half * 384, (half + 1) * 384)
+            share = dot(m.mix_high[:, inside], m.rows[inside, lines]) + dot(
+                m.mix_low[:, inside], m.rows[inside, lines]
+            )
+            if half == 0:
+                m.total[...] = share
+            else:
+                m.routed_out[:, lines] = (m.total[...] + share).astype(jnp.bfloat16)
 
     for near in [gate_near, up_near] + down_near:
         near.drain()
@@ -689,16 +770,16 @@
     operands = (
         second_micro_tokens,
         expert_norm_gain.reshape(1, -1),
-        routes,
-        visit_weight,
+        routes.T,
+        visit_weight.T,
         gate_weight_table,
         up_weight_table,
         down_weight_table,
         first_micro_values,
         group_state_maps,
         gate_preactivation,
-        step_preactivation,
-        decay_increment,
+        step_preactivation.T,
+        decay_increment.T,
         head_step_bias.reshape(1, -1),
         head_log_decay.reshape(1, -1),
         head_direct_gain.reshape(1, -1),

time: 207 us -> 180 us (0.87)
  Pallas kernels: 199 us -> 176 us
  local copies, waits for them, and re-layouts: 7.59 us -> 3.32 us
    pallas_call x1, Pallas kernels: 199 us -> 176 us  [body(): pl.pallas_call(kernel, out_shape=(jax.ShapeDtypeStruct((1024, 512), BF16)...]
    unnamed x16 -> x4, local copies, waits for them, and re-layouts: 7.59 us -> 3.32 us
where the time goes in v2:
time: 180 us
  Pallas kernels  176 us (98%)
  local copies, waits for them, and re-layouts  3.32 us (2%)
    pallas_call x1, Pallas kernels, body(): pl.pallas_call(kernel, out_shape=(jax.ShapeDtypeStruct((1024, 512), BF16)...  176 us

profile of v2, /device:TPU:1, one launch (start us, length us, event | category | flops | bytes accessed | tf_op | source)
XLA Modules:
  0.0 180.1 jit_solution(11922114295051653675)
XLA Ops:
  0.6 176.1 %shard_map.185 = (bf16[1024,512]{1,0:T(8,128)(2,1)}, bf16[256,2048]{1,0:T(8,128)(2,1)}) custom-call(bf16[256,2048]{1,0:T(8,128)(2,1)} %refs_0_.1, f32[1,2048]{1,0:T(1,128)} %bitcast.11, s32[2,256]{1,0:T(2,128)} %bitcast.12, f32[2,256]{1,0:T(2,128)} %bitcast.13, bf16[1,2048,256]{2,1,0:T(8,128)(2,1)} %refs_4_.1, bf16[1,2048,256]{2,1,0:T(8,128)(2,1)} %refs_5_.1, ...), custom_call_target="tpu_custom_call" | custom-call | tf_op jit(solution)/shard_map/pallas_call | solution.py:792
  176.8 0.0 copy-start
  176.8 2.4 %copy.22 = bf16[1024,512]{1,0:T(8,128)(2,1)} copy(bf16[1024,512]{1,0:T(8,128)(2,1)} %get-tuple-element.4) | data formatting | bytes 2097152
  179.1 0.0 copy-done
  179.1 1.0 copy.23
Async XLA Ops:
  176.8 2.4 %copy-start = (bf16[256,2048]{1,0:T(8,128)(2,1)S(1)}, bf16[256,2048]{1,0:T(8,128)(2,1)}, u32[]{:S(2)}) copy-start(bf16[256,2048]{1,0:T(8,128)(2,1)} %get-tuple-element.5) | copy-start | bytes 3145732

commit v3 on v2

--- a/solution.py
+++ b/solution.py
@@ -21,6 +21,7 @@
 
 
 SLOTS = 12
+CHUNKS = ((0, 512), (512, 512), (1024, 512), (1536, 512))
 ORDER = (4, 1, 7, 3, 5, 2, 6, 0)
 MESH_IDS = pl.DeviceIdType.MESH
 
@@ -436,9 +437,15 @@
     sent=pltpu.VMEM((64, 48, 512), BF16),
     landed=pltpu.VMEM((64, 48, 512), BF16),
     hidden=pltpu.VMEM((4, 768, 256), BF16),
-    answers=pltpu.VMEM((2, 64, 48, 256), BF16),
-    returned=pltpu.VMEM((2, 64, 48, 256), BF16),
-    total=pltpu.VMEM((256, 1024), F32),
+    answers_0=pltpu.VMEM((64, 48, 128), BF16),
+    answers_1=pltpu.VMEM((64, 48, 128), BF16),
+    answers_2=pltpu.VMEM((64, 48, 128), BF16),
+    answers_3=pltpu.VMEM((64, 48, 128), BF16),
+    returned_0=pltpu.VMEM((64, 48, 128), BF16),
+    returned_1=pltpu.VMEM((64, 48, 128), BF16),
+    returned_2=pltpu.VMEM((64, 48, 128), BF16),
+    returned_3=pltpu.VMEM((64, 48, 128), BF16),
+    total=pltpu.VMEM((256, 512), F32),
     gate_slots=pltpu.VMEM((4, 2048, 256), BF16),
     up_slots=pltpu.VMEM((4, 2048, 256), BF16),
     down_slots=pltpu.VMEM((4, 2048, 256), BF16),
@@ -468,8 +475,8 @@
     near_send=pltpu.SemaphoreType.DMA((24,)),
     near_recv=pltpu.SemaphoreType.DMA((24,)),
     dispatch_sems=pltpu.SemaphoreType.DMA((4,)),
-    answer_send=pltpu.SemaphoreType.DMA((4,)),
-    answer_recv=pltpu.SemaphoreType.DMA((4,)),
+    answer_send=pltpu.SemaphoreType.DMA((8,)),
+    answer_recv=pltpu.SemaphoreType.DMA((8,)),
     tail_send=pltpu.SemaphoreType.DMA((2,)),
     tail_recv=pltpu.SemaphoreType.DMA((2,)),
     plane_sems=pltpu.SemaphoreType.DMA((6,)),
@@ -510,17 +517,6 @@
     for step in (1, 3):
         greet(0, beside(step))
     for_all_peers(greet)
-    own_copies[0].wait()
-
-    def norm_rows(i, unused):
-        rows = pl.ds(pl.multiple_of(i * 32, 32), 32)
-        values = m.tokens[rows, :].astype(jnp.float32)
-        centered = values - jnp.mean(values, axis=1, keepdims=True)
-        scale = lax.rsqrt(jnp.mean(centered * centered, axis=1, keepdims=True) + EPSILON)
-        m.normed[rows, :] = (centered * scale * m.expert_gain[...]).astype(jnp.bfloat16)
-        return unused
-
-    lax.fori_loop(0, 8, norm_rows, 0)
     pl.semaphore_wait(barrier, 65)
 
     gate_near = Neighbours(m.gate_hbm, m.gate_slots, m.near_send, m.near_recv, 0, 0, 2048)
@@ -531,6 +527,7 @@
     ]
     gate_near.start()
     up_near.start()
+    down_near[0].start()
     after = lax.rem(me + 1, 64)
     tails = [
         pltpu.make_async_remote_copy(
@@ -554,6 +551,18 @@
     ]
     for copy in tails:
         copy.start()
+
+    own_copies[0].wait()
+
+    def norm_rows(i, unused):
+        rows = pl.ds(pl.multiple_of(i * 32, 32), 32)
+        values = m.tokens[rows, :].astype(jnp.float32)
+        centered = values - jnp.mean(values, axis=1, keepdims=True)
+        scale = lax.rsqrt(jnp.mean(centered * centered, axis=1, keepdims=True) + EPSILON)
+        m.normed[rows, :] = (centered * scale * m.expert_gain[...]).astype(jnp.bfloat16)
+        return unused
+
+    lax.fori_loop(0, 8, norm_rows, 0)
 
     experts = lax.broadcasted_iota(jnp.int32, (64, 256), 0)
     hits = [jnp.where(m.routes[k : k + 1, :] == experts, 1.0, 0.0) for k in range(2)]
@@ -647,16 +656,16 @@
         copy.wait()
     gate_near.forward()
     up_near.forward()
-    down_near[0].start()
+    down_near[0].forward()
     down_near[1].start()
+    down_near[2].start()
     states_second(m)
-    gate_near.arrive()
-    up_near.arrive()
-
-    def activate(half):
+
+    def gather(half):
         half_bytes(m.sent, m.landed, half, m.dispatch_sems.at[half], m.dispatch_sems.at[2 + half]).wait()
         unpack_half(m.landed, m.rows, matrix, half, 0, 512)
 
+    def activate(half, first, last):
         def one(j, unused):
             rows = m.rows[half * 384 : (half + 1) * 384, :]
             opened = dot(rows, m.gate_slots[j])
@@ -666,13 +675,17 @@
             )
             return unused
 
-        lax.fori_loop(0, 4, one, 0)
+        lax.fori_loop(first, last, one, 0)
+
+    answers = (m.answers_0, m.answers_1, m.answers_2, m.answers_3)
+    returned = (m.returned_0, m.returned_1, m.returned_2, m.returned_3)
 
     def answer(half, p):
         inside = slice(half * 384, (half + 1) * 384)
+        start, size = CHUNKS[p]
 
         def one(n, unused):
-            lines = pl.ds(pl.multiple_of(p * 1024 + n * 256, 256), 256)
+            lines = pl.ds(pl.multiple_of(start + n * 256, 256), 256)
             total = jnp.zeros((384, 256), jnp.float32)
             for j in range(4):
                 total = total + lax.dot_general(
@@ -684,62 +697,65 @@
             m.rows[inside, lines] = total.astype(jnp.bfloat16)
             return unused
 
-        lax.fori_loop(0, 4, one, 0)
+        lax.fori_loop(0, size // 256, one, 0)
         for g in range(half * 8, half * 8 + 8):
-            m.answers[p, g * 4 : g * 4 + 4] = pack_group(
-                m.rows[g * 48 : (g + 1) * 48, p * 1024 : (p + 1) * 1024], matrix, 256
+            answers[p][g * 4 : g * 4 + 4] = pack_group(
+                m.rows[g * 48 : (g + 1) * 48, start : start + size], matrix, size // 4
             )
         which = 2 * p + half
         sems = (m.answer_send.at[which], m.answer_recv.at[which])
         if half == 0:
-            m.returned[p, 7] = m.answers[p, 7]
-            send_group(m.answers.at[p], m.returned.at[p], 0, *sems, -1)
+            returned[p][7] = answers[p][7]
+            send_group(answers[p], returned[p], 0, *sems, -1)
 
         def some(dxc, unused):
-            send_group(m.answers.at[p], m.returned.at[p], dxc, *sems, -1)
+            send_group(answers[p], returned[p], dxc, *sems, -1)
             return unused
 
         lax.fori_loop(max(1, half * 4), half * 4 + 4, some, 0)
 
-    activate(0)
-    down_near[0].forward()
+    gather(0)
+    activate(0, 0, 3)
+    gate_near.arrive()
+    up_near.arrive()
+    activate(0, 3, 4)
+    down_near[0].arrive()
+    answer(0, 0)
+    gather(1)
+    activate(1, 0, 4)
+    answer(1, 0)
+    states_third(m)
     down_near[1].forward()
-    down_near[2].start()
     down_near[3].start()
-    activate(1)
-    states_third(m)
-    down_near[0].arrive()
     down_near[1].arrive()
-    answer(0, 0)
-    answer(1, 0)
+    answer(0, 1)
+    answer(1, 1)
     down_near[2].forward()
     down_near[3].forward()
     down_near[2].arrive()
+    answer(0, 2)
+    answer(1, 2)
     down_near[3].arrive()
-    answer(0, 1)
-    answer(1, 1)
+    answer(0, 3)
+    answer(1, 3)
     mixer_finish(m)
 
-    for p in range(2):
-        lines = pl.ds(p * 1024, 1024)
+    for p, (start, size) in enumerate(CHUNKS):
+        lines = pl.ds(start, size)
         for half in range(2):
             which = 2 * p + half
             half_bytes(
-                m.answers.at[p],
-                m.returned.at[p],
-                half,
-                m.answer_send.at[which],
-                m.answer_recv.at[which],
+                answers[p], returned[p], half, m.answer_send.at[which], m.answer_recv.at[which]
             ).wait()
-            unpack_half(m.returned.at[p], m.rows, matrix, half, p * 1024, 256)
+            unpack_half(returned[p], m.rows, matrix, half, start, size // 4)
             inside = slice(half * 384, (half + 1) * 384)
             share = dot(m.mix_high[:, inside], m.rows[inside, lines]) + dot(
                 m.mix_low[:, inside], m.rows[inside, lines]
             )
             if half == 0:
-                m.total[...] = share
+                m.total[:, 0:size] = share
             else:
-                m.routed_out[:, lines] = (m.total[...] + share).astype(jnp.bfloat16)
+                m.routed_out[:, lines] = (m.total[:, 0:size] + share).astype(jnp.bfloat16)
 
     for near in [gate_near, up_near] + down_near:
         near.drain()

time: 180 us -> 170 us (0.944)
  Pallas kernels: 176 us -> 166 us
    pallas_call x1, Pallas kernels: 176 us -> 166 us  [body(): pl.pallas_call(kernel, out_shape=(jax.ShapeDtypeStruct((1024, 512), BF16)...]
where the time goes in v3:
time: 170 us
  Pallas kernels  166 us (98%)
  local copies, waits for them, and re-layouts  3.32 us (2%)
    pallas_call x1, Pallas kernels, body(): pl.pallas_call(kernel, out_shape=(jax.ShapeDtypeStruct((1024, 512), BF16)...  166 us

profile of v3, /device:TPU:1, one launch (start us, length us, event | category | flops | bytes accessed | tf_op | source)
XLA Modules:
  0.0 170.1 jit_solution(9296373460792544243)
XLA Ops:
  0.6 166.1 %shard_map.185 = (bf16[1024,512]{1,0:T(8,128)(2,1)}, bf16[256,2048]{1,0:T(8,128)(2,1)}) custom-call(bf16[256,2048]{1,0:T(8,128)(2,1)} %refs_0_.1, f32[1,2048]{1,0:T(1,128)} %bitcast.11, s32[2,256]{1,0:T(2,128)} %bitcast.12, f32[2,256]{1,0:T(2,128)} %bitcast.13, bf16[1,2048,256]{2,1,0:T(8,128)(2,1)} %refs_4_.1, bf16[1,2048,256]{2,1,0:T(8,128)(2,1)} %refs_5_.1, ...), custom_call_target="tpu_custom_call" | custom-call | tf_op jit(solution)/shard_map/pallas_call | solution.py:808
  166.7 0.0 copy-start
  166.8 2.4 %copy.22 = bf16[1024,512]{1,0:T(8,128)(2,1)} copy(bf16[1024,512]{1,0:T(8,128)(2,1)} %get-tuple-element.4) | data formatting | bytes 2097152
  169.1 0.0 copy-done
  169.1 1.0 copy.23
Async XLA Ops:
  166.7 2.4 %copy-start = (bf16[256,2048]{1,0:T(8,128)(2,1)S(1)}, bf16[256,2048]{1,0:T(8,128)(2,1)}, u32[]{:S(2)}) copy-start(bf16[256,2048]{1,0:T(8,128)(2,1)} %get-tuple-element.5) | copy-start | bytes 3145732
